TPU v7x, 32 devices: a whole 2x2x4 slice. The times are simulated.
32 devices in a mesh: rep: 8 (over z, y), fs: 2 (over core), tp: 2 (over x).
Axes of the slice: x: 2, y: 2, z: 4, core: 2. Of those that a mesh axis runs over, the one named last changes fastest.
Arguments:
- inputs: bfloat16 [2048, 2048], P(('rep', 'fs'), 'tp'), may hold values from -6 to 6
- cotangent: bfloat16 [2048, 2048], P(('rep', 'fs'), 'tp'), may hold values from -6 to 6
- w_up: bfloat16 [2048, 4096], P('fs', 'tp'), may hold values from -0.125 to 0.125
- w_down: bfloat16 [4096, 2048], P('tp', 'fs'), may hold values from -0.09375 to 0.09375
Outputs:
- grad_inputs: bfloat16 [2048, 2048], P(('rep', 'fs'), 'tp')
- grad_up: float32 [2048, 4096], P('fs', 'tp')
- grad_down: float32 [4096, 2048], P('tp', 'fs')
All inputs are finite; a program needn't handle non-finite values.
Results may differ from a plain program's by a relative error of at most 0.011.
Values may be sent and summed in bfloat16 or wider, within the bound.
No kernel may reach another device: no remote copies, remote signals or barrier semaphores. Data moves between devices by JAX's collectives and lax.ppermute only.
A program may use at most 128 MiB of HBM per device.

v0:
```python
import functools

import jax
import jax.numpy as jnp
from jax import lax
from jax.experimental import pallas as pl
from jax.experimental.pallas import tpu as pltpu
from jax.sharding import PartitionSpec as P


BF16, F32 = jnp.bfloat16, jnp.float32
VMEM = pl.BlockSpec(memory_space=pltpu.VMEM)
SMEM = pl.BlockSpec(memory_space=pltpu.SMEM)
HBM = pl.BlockSpec(memory_space=pltpu.HBM)
MIB = 1 << 20


def dot(left, right, contract):
    return lax.dot_general(left, right, (contract, ((), ())), preferred_element_type=F32)


def tile_of(size):
    return 512 if size % 512 == 0 else size


def folded_ring(length):
    return [0] + list(range(1, length, 2)) + list(range(length - 2 + length % 2, 0, -2))


def plan(n_rep, tokens_each, hidden):
    group = n_rep
    while group > 2 and (n_rep % group or group % 2 or group * tokens_each > hidden):
        group -= 1
    return group


def ready_kernel(flag_ref, up_ref, down_ref, out_ref):
    out_ref[0] = flag_ref[0]


def ready(flag, w_up, w_down):
    return pl.pallas_call(
        ready_kernel,
        in_specs=[SMEM, VMEM, VMEM],
        out_specs=SMEM,
        out_shape=jax.ShapeDtypeStruct((1,), jnp.int32),
        compiler_params=pltpu.CompilerParams(vmem_limit_bytes=10 * MIB),
        name="ready",
    )(flag, w_up, w_down)


def forward_kernel(count, first, same_ref, *refs):
    mine, theirs = refs[:count], refs[count : 2 * count]
    up_ref, down_ref, up_other, down_other = refs[2 * count : 2 * count + 4]
    packet_ref, keep_ref, *part_ref = refs[2 * count + 4 : 2 * count + 6 + first]
    give_ref, up_buf, down_buf, sems, *sum_ref = refs[2 * count + 6 + first :]
    _, rows, _ = mine[0].shape
    hidden, tile = up_ref.shape[1], up_buf.shape[2]
    steps = hidden // tile

    def copy(step, which):
        slot = lax.rem(step, 2)
        cols = pl.ds(pl.multiple_of(step * tile, tile), tile)
        if which == 0:
            source, target = up_other.at[:, cols], up_buf.at[slot]
        else:
            source, target = down_other.at[cols, :], down_buf.at[slot]
        return pltpu.make_async_copy(source, target, sems.at[slot, which])

    for which in range(2):
        copy(0, which).start()

    def choose(kept, given):
        for at in range(count):
            place = pl.ds(at * rows, rows)
            keep_ref[:, place, :] = kept[at][...]
            give_ref[:, place, :] = given[at][...]
            packet_ref[:, place, hidden:] = given[at][...]

    if first:
        sum_ref[0][...] = jnp.zeros_like(sum_ref[0])
    same = same_ref[0] == 1

    @pl.when(same)
    def _():
        choose(mine, theirs)

    @pl.when(jnp.logical_not(same))
    def _():
        choose(theirs, mine)

    @pl.loop(0, steps)
    def _(step):
        slot = lax.rem(step, 2)
        cols = pl.ds(pl.multiple_of(step * tile, tile), tile)

        @pl.when(step + 1 < steps)
        def _():
            for which in range(2):
                copy(step + 1, which).start()

        for which in range(2):
            copy(step, which).wait()
        preact = dot(keep_ref[0], up_ref[:, cols], ((1,), (0,)))
        preact += dot(give_ref[0], up_buf[slot], ((1,), (0,)))
        act_grad = dot(keep_ref[1], down_ref[cols, :], ((1,), (1,)))
        act_grad += dot(give_ref[1], down_buf[slot], ((1,), (1,)))
        relu_pre = jnp.maximum(preact, 0.0)
        pre_grad = (2.0 * relu_pre * act_grad).astype(BF16)
        packet_ref[0, :, cols] = pre_grad
        packet_ref[1, :, cols] = (relu_pre * relu_pre).astype(BF16)
        if first:
            for at, held in enumerate((up_ref[:, cols], up_buf[slot])):
                sum_ref[0][at] += dot(pre_grad[:rows], held, ((1,), (1,)))

    if first:
        part_ref[0][1 - same_ref[0]] = sum_ref[0][0].astype(BF16)
        part_ref[0][same_ref[0]] = sum_ref[0][1].astype(BF16)


def forward(same, mine, theirs, weights, first):
    count = len(mine)
    _, rows, part = mine[0].shape
    hidden = weights[0].shape[1]
    tokens, tile = count * rows, tile_of(hidden)
    return pl.pallas_call(
        functools.partial(forward_kernel, count, first),
        in_specs=[SMEM] + [VMEM] * (2 * count + 2) + [HBM] * 2,
        out_specs=[VMEM] * (2 + first),
        out_shape=[
            jax.ShapeDtypeStruct((2, tokens, hidden + part), BF16),
            jax.ShapeDtypeStruct((2, tokens, part), BF16),
            jax.ShapeDtypeStruct((2, rows, part), BF16),
        ][: 2 + first],
        scratch_shapes=[
            pltpu.VMEM((2, tokens, part), BF16),
            pltpu.VMEM((2, part, tile), BF16),
            pltpu.VMEM((2, tile, part), BF16),
            pltpu.SemaphoreType.DMA((2, 2)),
            pltpu.VMEM((2, rows, part), F32),
        ][: 4 + first],
        compiler_params=pltpu.CompilerParams(vmem_limit_bytes=11 * MIB),
        cost_estimate=pl.CostEstimate(
            flops=8 * tokens * part * hidden, bytes_accessed=8 * part * hidden, transcendentals=0
        ),
        name="forward",
    )(same, *mine, *theirs, *weights)


def grads_of(pieces, cols, hidden):
    def rows(which):
        parts = []
        for keep, packet, got in pieces:
            parts += [packet[which, :, cols], got[which, :, cols]]
        return jnp.concatenate(parts, axis=0)

    def tokens(which):
        parts = []
        for keep, packet, got in pieces:
            parts += [keep[which], got[which, :, hidden:]]
        return jnp.concatenate(parts, axis=0)

    up = dot(tokens(0), rows(0), ((0,), (0,)))
    return up, dot(rows(1), tokens(1), ((0,), (0,)))


def triples(refs, count):
    return [refs[3 * at : 3 * at + 3] for at in range(count)]


def accumulate_kernel(count, first, last, *refs):
    pieces = triples(refs, count)
    up_ref, down_ref = refs[-2:]
    up_in, down_in = (None, None) if first else refs[3 * count : 3 * count + 2]
    hidden = down_ref.shape[0] if first else down_in.shape[0]
    tile = down_ref.shape[0] if last else tile_of(hidden)

    def add(step, up_to, down_to):
        cols = pl.ds(pl.multiple_of(step * tile, tile), tile)
        up, down = grads_of(pieces, cols, hidden)
        if not first:
            up, down = up_in[:, cols].astype(F32) + up, down_in[cols, :].astype(F32) + down
        up_ref[:, up_to(cols)] = up.astype(up_ref.dtype)
        down_ref[down_to(cols), :] = down.astype(down_ref.dtype)

    if last:
        add(pl.program_id(0), lambda cols: slice(None), lambda cols: slice(None))
    else:
        pl.loop(0, hidden // tile)(lambda step: add(step, lambda cols: cols, lambda cols: cols))


def accumulate(pieces, sums, last):
    keep, packet, _ = pieces[0]
    tokens = sum(piece[0].shape[1] for piece in pieces)
    part = keep.shape[2]
    hidden = packet.shape[2] - part
    tile = tile_of(hidden)
    args = [array for piece in pieces for array in piece] + list(sums or ())
    how = dict(
        in_specs=[VMEM] * len(args),
        out_specs=[VMEM, VMEM],
        out_shape=[
            jax.ShapeDtypeStruct((part, hidden), F32 if last else BF16),
            jax.ShapeDtypeStruct((hidden, part), F32 if last else BF16),
        ],
        compiler_params=pltpu.CompilerParams(vmem_limit_bytes=(16 if last else 9) * MIB),
        cost_estimate=pl.CostEstimate(
            flops=8 * tokens * part * hidden, bytes_accessed=8 * part * hidden, transcendentals=0
        ),
        name="accumulate",
    )
    if last:
        how |= dict(
            grid=(hidden // tile,),
            out_specs=[
                pl.BlockSpec((part, tile), lambda j: (0, j)),
                pl.BlockSpec((tile, part), lambda j: (j, 0)),
            ],
        )
    elif sums is not None:
        how |= dict(input_output_aliases={len(args) - 2: 0, len(args) - 1: 1})
    return pl.pallas_call(
        functools.partial(accumulate_kernel, len(pieces), sums is None, last), **how
    )(*args)


def build(mesh):
    n_rep, n_fs, _ = (mesh.shape[name] for name in ("rep", "fs", "tp"))

    def shards(inputs, cotangent, w_up, w_down):
        rows, _ = inputs.shape
        group = plan(n_rep, rows * n_fs, w_up.shape[1])
        length = group // 2
        ring = folded_ring(length)
        follows = {ring[i]: ring[(i + 1) % length] for i in range(length)}
        along = [
            (base * group + 2 * at + side, base * group + 2 * follows[at] + side)
            for base in range(n_rep // group)
            for at in range(length)
            for side in range(2)
        ]
        back = [(target, source) for source, target in along]
        across = [(place, place ^ 1) for place in range(n_rep)]
        swap = [(0, 1), (1, 0)]

        same = lax.axis_index("fs") == lax.axis_index("tp")
        flag = same.astype(jnp.int32)[None]

        near = [jnp.stack([inputs, cotangent])]
        beside, over, corner = [], [], {}
        other_up = lax.ppermute(w_up, "fs", swap)
        other_down = lax.ppermute(w_down, "fs", swap)
        weights = (w_up, w_down, other_up, other_down)
        flag = ready(flag, w_up, w_down)
        for step in range(length):
            beside.append(lax.ppermute(near[step], "tp", swap))
            over.append(lax.ppermute(near[step], "rep", across))
            if step == 0:
                corner[0] = lax.ppermute(beside[0], "rep", across)
            if step + 1 < length:
                near.append(lax.ppermute(near[step], "rep", along))
        for step in range(length - 1, 1, -1):
            corner[step] = lax.ppermute(corner[(step + 1) % length], "rep", back)
        if length > 1:
            corner[1] = lax.ppermute(over[1], "tp", swap)
        own = [(near[k], beside[k]) for k in range(length)]
        far = [(over[k], corner[k]) for k in range(length)]
        groups = {f"o{k}": group for k, group in enumerate(own)}
        groups |= {f"f{k}": group for k, group in enumerate(far)}

        made = []
        for at, names in enumerate(CHUNKS):
            packet, keep, *partial_value = forward(
                flag, *zip(*(groups[name] for name in names)), weights, at == 0
            )
            if at == 0:
                partial_here, partial_there = partial_value[0]
            made.append((keep, packet, lax.ppermute(packet, "fs", swap)))
        sums = None
        for at, chunks in enumerate(BATCHES):
            sums = accumulate([made[k] for k in chunks], sums, at == len(BATCHES) - 1)
        grad_up, grad_down = sums

        passed = lax.ppermute(partial_there, "tp", swap)
        grad_inputs = (partial_here.astype(F32) + passed.astype(F32)).astype(BF16)
        if n_rep > group:
            sets = [[base * group + at for base in range(n_rep // group)] for at in range(group)]
            grad_up, grad_down = (
                lax.psum(t, "rep", axis_index_groups=sets) for t in (grad_up, grad_down)
            )
        return (grad_inputs, grad_up, grad_down)

    return shards


CHUNKS = (("o0",), ("o1", "f0"), ("o2", "o3"), ("f3", "f1", "f2"))
BATCHES = ((0, 1), (2,), (3,))


def solution(mesh):
    run = build(mesh)

    return jax.shard_map(
        run,
        mesh=mesh,
        in_specs=(P(("rep", "fs"), "tp"), P(("rep", "fs"), "tp"), P("fs", "tp"), P("tp", "fs")),
        out_specs=(P(("rep", "fs"), "tp"), P("fs", "tp"), P("tp", "fs")),
        check_vma=False,
    )
```

profile of v0, /device:TPU:0, one launch (start us, length us, event | category | flops | bytes accessed | tf_op | source)
XLA Modules:
  0.0 158.3 jit_solution(5484806998756944861)
XLA Ops:
  1.3 1.1 pad_maximum_fusion.refs_0_
  2.4 3.0 %collective-permute-start.4 = (bf16[2,128,1024]{2,1,0:T(8,128)(2,1)S(1)}, bf16[2,128,1024]{2,1,0:T(8,128)(2,1)S(1)}, u32[]{:S(2)}, u32[]{:S(2)}) collective-permute-start(bf16[2,128,1024]{2,1,0:T(8,128)(2,1)S(1)} %pad_maximum_fusion.refs_0_), channel_id=1, source_target_pairs={{0,8},{4,12},{8,24},{12,28},{16,0},{20,4},{24,16},{28,20},{1,9},{5... | collective-permute-start | bytes 1572872 | tf_op jit(solution)/shard_map/ppermute | solution.py:261
  5.4 1.5 collective-permute-start
  6.9 11.7 %collective-permute-done.4.refs_0_ = bf16[2,128,1024]{2,1,0:T(8,128)(2,1)S(1)} collective-permute-done((bf16[2,128,1024]{2,1,0:T(8,128)(2,1)S(1)}, bf16[2,128,1024]{2,1,0:T(8,128)(2,1)S(1)}, u32[]{:S(2)}, u32[]{:S(2)}) %collective-permute-start.4) | collective-permute-done | bytes 524320 | tf_op jit(solution)/shard_map/ppermute | solution.py:261
  18.6 1.6 collective-permute-start.8
  21.4 11.9 %collective-permute-done.8.refs_1_ = bf16[2,128,1024]{2,1,0:T(8,128)(2,1)S(1)} collective-permute-done((bf16[2,128,1024]{2,1,0:T(8,128)(2,1)S(1)}, bf16[2,128,1024]{2,1,0:T(8,128)(2,1)S(1)}, u32[]{:S(2)}, u32[]{:S(2)}) %collective-permute-start.8) | collective-permute-done | bytes 524320 | tf_op jit(solution)/shard_map/ppermute | solution.py:257
  33.4 1.5 collective-permute-start.12
  34.9 0.8 copy-done.3
  36.5 6.7 %collective-permute-done.10.refs_3_ = bf16[2,128,1024]{2,1,0:T(8,128)(2,1)S(1)} collective-permute-done((bf16[2,128,1024]{2,1,0:T(8,128)(2,1)S(1)}, bf16[2,128,1024]{2,1,0:T(8,128)(2,1)S(1)}, u32[]{:S(2)}, u32[]{:S(2)}) %collective-permute-start.10) | collective-permute-done | bytes 524320 | tf_op jit(solution)/shard_map/ppermute | solution.py:259
  43.1 1.5 collective-permute-start.11
  44.6 0.8 copy-done.5
  45.4 1.5 collective-permute-start.9
  46.9 0.9 collective-permute-done.6.refs_1_
  47.8 1.6 %collective-permute-start.7 = (bf16[2,128,1024]{2,1,0:T(8,128)(2,1)S(1)}, bf16[2,128,1024]{2,1,0:T(8,128)(2,1)}, u32[]{:S(2)}, u32[]{:S(2)}) collective-permute-start(bf16[2,128,1024]{2,1,0:T(8,128)(2,1)S(1)} %collective-permute-done.6.refs_1_), channel_id=1, source_target_pairs={{0,4},{4,0},{8,12},{12,8},{16,20},{20,16},{24,28},{28,24},{1,5},{5... | collective-permute-start | bytes 1572872 | tf_op jit(solution)/shard_map/ppermute | solution.py:257
  49.4 8.7 %collective-permute-done.11.refs_3_ = bf16[2,128,1024]{2,1,0:T(8,128)(2,1)} collective-permute-done((bf16[2,128,1024]{2,1,0:T(8,128)(2,1)S(1)}, bf16[2,128,1024]{2,1,0:T(8,128)(2,1)}, u32[]{:S(2)}, u32[]{:S(2)}) %collective-permute-start.11) | collective-permute-done | bytes 524320 | tf_op jit(solution)/shard_map/ppermute | solution.py:263
  58.1 0.9 collective-permute-start.13
  59.0 2.2 %copy-done = bf16[1024,2048]{1,0:T(8,128)(2,1)S(1)} copy-done((bf16[1024,2048]{1,0:T(8,128)(2,1)S(1)}, bf16[1024,2048]{1,0:T(8,128)(2,1)}, u32[]{:S(2)}) %copy-start) | copy-done | bytes 4194328
  61.2 2.2 %copy-done.2 = bf16[2048,1024]{1,0:T(8,128)(2,1)S(1)} copy-done((bf16[2048,1024]{1,0:T(8,128)(2,1)S(1)}, bf16[2048,1024]{1,0:T(8,128)(2,1)}, u32[]{:S(2)}) %copy-start.2) | copy-done | bytes 4194328
  63.9 1.6 %collective-permute-start.19 = (bf16[2,128,1024]{2,1,0:T(8,128)(2,1)S(1)}, bf16[2,128,1024]{2,1,0:T(8,128)(2,1)S(1)}, u32[]{:S(2)}, u32[]{:S(2)}) collective-permute-start(bf16[2,128,1024]{2,1,0:T(8,128)(2,1)S(1)} %pad_maximum_fusion.refs_0_), channel_id=1, source_target_pairs={{0,4},{4,0},{8,12},{12,8},{16,20},{20,16},{24,28},{28,24},{1,5},{5... | collective-permute-start | bytes 1572872 | tf_op jit(solution)/shard_map/ppermute | solution.py:257
  65.5 6.0 %collective-permute-done.7.refs_0_ = bf16[2,128,1024]{2,1,0:T(8,128)(2,1)} collective-permute-done((bf16[2,128,1024]{2,1,0:T(8,128)(2,1)S(1)}, bf16[2,128,1024]{2,1,0:T(8,128)(2,1)}, u32[]{:S(2)}, u32[]{:S(2)}) %collective-permute-start.7) | collective-permute-done | bytes 524320 | tf_op jit(solution)/shard_map/ppermute | solution.py:257
  71.5 1.5 collective-permute-start.20
  73.1 10.9 %forward.5 = (bf16[2,384,3072]{2,1,0:T(8,128)(2,1)S(1)}, bf16[2,384,1024]{2,1,0:T(8,128)(2,1)S(1)}) custom-call(s32[1]{0:T(128)} %ready.1.same_ref, bf16[2,128,1024]{2,1,0:T(8,128)(2,1)} %collective-permute-done.7.refs_0_, bf16[2,128,1024]{2,1,0:T(8,128)(2,1)S(1)} %copy-done.4, bf16[2,128,1024]{2,1,0:T(8,128)(2,1)} %collective-permute-done.9.refs_2_, ...), custom_call_target="tpu_custom_call" | custom-call | flops 6442450944 | bytes 16777216 | tf_op jit(solution)/shard_map/forward/pallas_call | solution.py:126
  84.7 1.5 collective-permute-start.16
  86.2 7.6 %forward.7 = (bf16[2,256,3072]{2,1,0:T(8,128)(2,1)S(1)}, bf16[2,256,1024]{2,1,0:T(8,128)(2,1)S(1)}) custom-call(s32[1]{0:T(128)} %ready.1.same_ref, bf16[2,128,1024]{2,1,0:T(8,128)(2,1)S(1)} %collective-permute-done.4.refs_0_, bf16[2,128,1024]{2,1,0:T(8,128)(2,1)S(1)} %collective-permute-done.19.refs_1_, ...), custom_call_target="tpu_custom_call" | custom-call | flops 4294967296 | bytes 16777216 | tf_op jit(solution)/shard_map/forward/pallas_call | solution.py:126
  93.9 5.1 %collective-permute-done.15.refs_2_ = bf16[2,128,1024]{2,1,0:T(8,128)(2,1)S(1)} collective-permute-done((bf16[2,128,1024]{2,1,0:T(8,128)(2,1)S(1)}, bf16[2,128,1024]{2,1,0:T(8,128)(2,1)S(1)}, u32[]{:S(2)}, u32[]{:S(2)}) %collective-permute-start.15) | collective-permute-done | bytes 524320 | tf_op jit(solution)/shard_map/ppermute | solution.py:256
  98.9 10.7 %collective-permute-done.16.refs_3_ = bf16[2,128,1024]{2,1,0:T(8,128)(2,1)S(1)} collective-permute-done((bf16[2,128,1024]{2,1,0:T(8,128)(2,1)S(1)}, bf16[2,128,1024]{2,1,0:T(8,128)(2,1)S(1)}, u32[]{:S(2)}, u32[]{:S(2)}) %collective-permute-start.16) | collective-permute-done | bytes 524320 | tf_op jit(solution)/shard_map/ppermute | solution.py:256
  109.6 7.6 %forward.6 = (bf16[2,256,3072]{2,1,0:T(8,128)(2,1)S(1)}, bf16[2,256,1024]{2,1,0:T(8,128)(2,1)S(1)}) custom-call(s32[1]{0:T(128)} %ready.1.same_ref, bf16[2,128,1024]{2,1,0:T(8,128)(2,1)S(1)} %collective-permute-done.5.refs_0_, bf16[2,128,1024]{2,1,0:T(8,128)(2,1)S(1)} %collective-permute-done.6.refs_1_, ...), custom_call_target="tpu_custom_call" | custom-call | flops 4294967296 | bytes 16777216 | tf_op jit(solution)/shard_map/forward/pallas_call | solution.py:126
  117.3 9.6 %forward.4 = (bf16[2,128,3072]{2,1,0:T(8,128)(2,1)S(1)}, bf16[2,128,1024]{2,1,0:T(8,128)(2,1)S(1)}, bf16[2,128,1024]{2,1,0:T(8,128)(2,1)S(1)}) custom-call(s32[1]{0:T(128)} %ready.1.same_ref, bf16[2,128,1024]{2,1,0:T(8,128)(2,1)S(1)} %pad_maximum_fusion.refs_0_, bf16[2,128,1024]{2,1,0:T(8,128)(2,1)S(1)} %collective-permute-done.refs_1_, ...), custom_call_target="tpu_custom_call" | custom-call | flops 2147483648 | bytes 16777216 | tf_op jit(solution)/shard_map/forward/pallas_call | solution.py:126
  128.1 7.7 %collective-permute-done.3 = bf16[128,1024]{1,0:T(8,128)(2,1)S(1)} collective-permute-done((bf16[128,1024]{1,0:T(8,128)(2,1)S(1)}, bf16[128,1024]{1,0:T(8,128)(2,1)S(1)}, u32[]{:S(2)}, u32[]{:S(2)}) %collective-permute-start.3) | collective-permute-done | bytes 262176 | tf_op jit(solution)/shard_map/ppermute | solution.py:284
  136.6 7.4 %accumulate.3 = (bf16[1024,2048]{1,0:T(8,128)(2,1)S(1)}, bf16[2048,1024]{1,0:T(8,128)(2,1)S(1)}) custom-call(bf16[2,128,1024]{2,1,0:T(8,128)(2,1)S(1)} %get-tuple-element.23.refs_0_, bf16[2,128,3072]{2,1,0:T(8,128)(2,1)S(1)} %get-tuple-element.24.refs_1_, bf16[2,128,3072]{2,1,0:T(8,128)(2,1)S(1)} %collective-permute-done.18.refs_2_, ...), custom_call_target="tpu_custom_call" | custom-call | flops 6442450944 | bytes 16777216 | tf_op jit(solution)/shard_map/accumulate/pallas_call | solution.py:222
  144.0 5.5 %accumulate.4 = (bf16[1024,2048]{1,0:T(8,128)(2,1)S(1)}, bf16[2048,1024]{1,0:T(8,128)(2,1)S(1)}) custom-call(bf16[2,256,1024]{2,1,0:T(8,128)(2,1)S(1)} %get-tuple-element.21.refs_0_, bf16[2,256,3072]{2,1,0:T(8,128)(2,1)S(1)} %get-tuple-element.22.refs_1_, ...), custom_call_target="tpu_custom_call", output_to_operand_aliasing={{0}: (3, {}), {1}: (4, {})} | custom-call | flops 4294967296 | bytes 16777216 | tf_op jit(solution)/shard_map/accumulate/pallas_call | solution.py:222
  149.5 8.8 %accumulate.5 = (f32[1024,2048]{1,0:T(8,128)}, f32[2048,1024]{1,0:T(8,128)}) custom-call(bf16[2,384,1024]{2,1,0:T(8,128)(2,1)S(1)} %get-tuple-element.19.refs_0_, bf16[2,384,3072]{2,1,0:T(8,128)(2,1)S(1)} %get-tuple-element.20.refs_1_, bf16[2,384,3072]{2,1,0:T(8,128)(2,1)S(1)} %collective-permute-done.14.refs_2_, ...), custom_call_target="tpu_custom_call" | custom-call | flops 6442450944 | bytes 16777216 | tf_op jit(solution)/shard_map/accumulate/pallas_call | solution.py:222
  (37 shorter events, 6.0 us)
Async XLA Ops:
  0.6 72.4 %collective-permute-start.1 = (bf16[1024,2048]{1,0:T(8,128)(2,1)}, bf16[1024,2048]{1,0:T(8,128)(2,1)}, u32[]{:S(2)}, u32[]{:S(2)}) collective-permute-start(bf16[1024,2048]{1,0:T(8,128)(2,1)} %refs_4_.3), channel_id=1, source_target_pairs={{0,2},{2,0},{1,3},{3,1},{4,6},{6,4},{5,7},{7,5},{8,10},{10,8},{9,1... | collective-permute-start | bytes 12582920 | tf_op jit(solution)/shard_map/ppermute | solution.py:251
  1.2 71.9 %collective-permute-start.2 = (bf16[2048,1024]{1,0:T(8,128)(2,1)}, bf16[2048,1024]{1,0:T(8,128)(2,1)}, u32[]{:S(2)}, u32[]{:S(2)}) collective-permute-start(bf16[2048,1024]{1,0:T(8,128)(2,1)} %refs_5_.3), channel_id=1, source_target_pairs={{0,2},{2,0},{1,3},{3,1},{4,6},{6,4},{5,7},{7,5},{8,10},{10,8},{9,1... | collective-permute-start | bytes 12582920 | tf_op jit(solution)/shard_map/ppermute | solution.py:252
  2.4 16.2 %collective-permute-start.4 = (bf16[2,128,1024]{2,1,0:T(8,128)(2,1)S(1)}, bf16[2,128,1024]{2,1,0:T(8,128)(2,1)S(1)}, u32[]{:S(2)}, u32[]{:S(2)}) collective-permute-start(bf16[2,128,1024]{2,1,0:T(8,128)(2,1)S(1)} %pad_maximum_fusion.refs_0_), channel_id=1, source_target_pairs={{0,8},{4,12},{8,24},{12,28},{16,0},{20,4},{24,16},{28,20},{1,9},{5... | collective-permute-start | bytes 1572872 | tf_op jit(solution)/shard_map/ppermute | solution.py:261
  5.4 15.5 %collective-permute-start = (bf16[2,128,1024]{2,1,0:T(8,128)(2,1)S(1)}, bf16[2,128,1024]{2,1,0:T(8,128)(2,1)S(1)}, u32[]{:S(2)}, u32[]{:S(2)}) collective-permute-start(bf16[2,128,1024]{2,1,0:T(8,128)(2,1)S(1)} %pad_maximum_fusion.refs_0_), channel_id=1, source_target_pairs={{0,1},{1,0},{2,3},{3,2},{4,5},{5,4},{6,7},{7,6},{8,9},{9,8},{10,11... | collective-permute-start | bytes 1572872 | tf_op jit(solution)/shard_map/ppermute | solution.py:256
  18.6 14.8 %collective-permute-start.8 = (bf16[2,128,1024]{2,1,0:T(8,128)(2,1)S(1)}, bf16[2,128,1024]{2,1,0:T(8,128)(2,1)S(1)}, u32[]{:S(2)}, u32[]{:S(2)}) collective-permute-start(bf16[2,128,1024]{2,1,0:T(8,128)(2,1)S(1)} %collective-permute-done.4.refs_0_), channel_id=1, source_target_pairs={{0,4},{4,0},{8,12},{12,8},{16,20},{20,16},{24,28},{28,24},{1,5},{5... | collective-permute-start | bytes 1572872 | tf_op jit(solution)/shard_map/ppermute | solution.py:257
  20.1 15.6 %collective-permute-start.5 = (bf16[2,128,1024]{2,1,0:T(8,128)(2,1)S(1)}, bf16[2,128,1024]{2,1,0:T(8,128)(2,1)S(1)}, u32[]{:S(2)}, u32[]{:S(2)}) collective-permute-start(bf16[2,128,1024]{2,1,0:T(8,128)(2,1)S(1)} %collective-permute-done.4.refs_0_), channel_id=1, source_target_pairs={{0,8},{4,12},{8,24},{12,28},{16,0},{20,4},{24,16},{28,20},{1,9},{5... | collective-permute-start | bytes 1572872 | tf_op jit(solution)/shard_map/ppermute | solution.py:261
  20.9 22.2 %collective-permute-start.10 = (bf16[2,128,1024]{2,1,0:T(8,128)(2,1)S(1)}, bf16[2,128,1024]{2,1,0:T(8,128)(2,1)S(1)}, u32[]{:S(2)}, u32[]{:S(2)}) collective-permute-start(bf16[2,128,1024]{2,1,0:T(8,128)(2,1)S(1)} %collective-permute-done.refs_1_), channel_id=1, source_target_pairs={{0,4},{4,0},{8,12},{12,8},{16,20},{20,16},{24,28},{28,24},{1,5},{5... | collective-permute-start | bytes 1572872 | tf_op jit(solution)/shard_map/ppermute | solution.py:259
  33.4 11.2 %collective-permute-start.12 = (bf16[2,128,1024]{2,1,0:T(8,128)(2,1)S(1)}, bf16[2,128,1024]{2,1,0:T(8,128)(2,1)S(1)}, u32[]{:S(2)}, u32[]{:S(2)}) collective-permute-start(bf16[2,128,1024]{2,1,0:T(8,128)(2,1)S(1)} %collective-permute-done.8.refs_1_), channel_id=1, source_target_pairs={{0,1},{1,0},{2,3},{3,2},{4,5},{5,4},{6,7},{7,6},{8,9},{9,8},{10,11... | collective-permute-start | bytes 1572872 | tf_op jit(solution)/shard_map/ppermute | solution.py:265
  34.9 0.8 copy-start.3
  35.7 12.1 %collective-permute-start.6 = (bf16[2,128,1024]{2,1,0:T(8,128)(2,1)S(1)}, bf16[2,128,1024]{2,1,0:T(8,128)(2,1)S(1)}, u32[]{:S(2)}, u32[]{:S(2)}) collective-permute-start(bf16[2,128,1024]{2,1,0:T(8,128)(2,1)S(1)} %collective-permute-done.5.refs_0_), channel_id=1, source_target_pairs={{0,8},{4,12},{8,24},{12,28},{16,0},{20,4},{24,16},{28,20},{1,9},{5... | collective-permute-start | bytes 1572872 | tf_op jit(solution)/shard_map/ppermute | solution.py:261
  43.1 15.0 %collective-permute-start.11 = (bf16[2,128,1024]{2,1,0:T(8,128)(2,1)S(1)}, bf16[2,128,1024]{2,1,0:T(8,128)(2,1)}, u32[]{:S(2)}, u32[]{:S(2)}) collective-permute-start(bf16[2,128,1024]{2,1,0:T(8,128)(2,1)S(1)} %collective-permute-done.10.refs_3_), channel_id=1, source_target_pairs={{8,0},{12,4},{24,8},{28,12},{0,16},{4,20},{16,24},{20,28},{9,1},{1... | collective-permute-start | bytes 1572872 | tf_op jit(solution)/shard_map/ppermute | solution.py:263
  44.6 0.8 copy-start.5
  45.4 18.5 %collective-permute-start.9 = (bf16[2,128,1024]{2,1,0:T(8,128)(2,1)S(1)}, bf16[2,128,1024]{2,1,0:T(8,128)(2,1)}, u32[]{:S(2)}, u32[]{:S(2)}) collective-permute-start(bf16[2,128,1024]{2,1,0:T(8,128)(2,1)S(1)} %collective-permute-done.5.refs_0_), channel_id=1, source_target_pairs={{0,4},{4,0},{8,12},{12,8},{16,20},{20,16},{24,28},{28,24},{1,5},{5... | collective-permute-start | bytes 1572872 | tf_op jit(solution)/shard_map/ppermute | solution.py:257
  47.8 23.7 %collective-permute-start.7 = (bf16[2,128,1024]{2,1,0:T(8,128)(2,1)S(1)}, bf16[2,128,1024]{2,1,0:T(8,128)(2,1)}, u32[]{:S(2)}, u32[]{:S(2)}) collective-permute-start(bf16[2,128,1024]{2,1,0:T(8,128)(2,1)S(1)} %collective-permute-done.6.refs_1_), channel_id=1, source_target_pairs={{0,4},{4,0},{8,12},{12,8},{16,20},{20,16},{24,28},{28,24},{1,5},{5... | collective-permute-start | bytes 1572872 | tf_op jit(solution)/shard_map/ppermute | solution.py:257
  58.1 14.9 %collective-permute-start.13 = (bf16[2,128,1024]{2,1,0:T(8,128)(2,1)}, bf16[2,128,1024]{2,1,0:T(8,128)(2,1)}, u32[]{:S(2)}, u32[]{:S(2)}) collective-permute-start(bf16[2,128,1024]{2,1,0:T(8,128)(2,1)} %collective-permute-done.11.refs_3_), channel_id=1, source_target_pairs={{8,0},{12,4},{24,8},{28,12},{0,16},{4,20},{16,24},{20,28},{9,1},{1... | collective-permute-start | bytes 1572872 | tf_op jit(solution)/shard_map/ppermute | solution.py:263
  59.0 2.2 %copy-start = (bf16[1024,2048]{1,0:T(8,128)(2,1)S(1)}, bf16[1024,2048]{1,0:T(8,128)(2,1)}, u32[]{:S(2)}) copy-start(bf16[1024,2048]{1,0:T(8,128)(2,1)} %refs_4_.3) | copy-start | bytes 12582916
  61.2 2.2 %copy-start.2 = (bf16[2048,1024]{1,0:T(8,128)(2,1)S(1)}, bf16[2048,1024]{1,0:T(8,128)(2,1)}, u32[]{:S(2)}) copy-start(bf16[2048,1024]{1,0:T(8,128)(2,1)} %refs_5_.3) | copy-start | bytes 12582916
  63.4 9.7 %copy-start.1 = (bf16[1024,2048]{1,0:T(8,128)(2,1)S(1)}, bf16[1024,2048]{1,0:T(8,128)(2,1)}, u32[]{:S(2)}) copy-start(bf16[1024,2048]{1,0:T(8,128)(2,1)} %refs_4_.3) | copy-start | bytes 12582916
  63.4 9.7 %copy-start.4 = (bf16[2,128,1024]{2,1,0:T(8,128)(2,1)S(1)}, bf16[2,128,1024]{2,1,0:T(8,128)(2,1)}, u32[]{:S(2)}) copy-start(bf16[2,128,1024]{2,1,0:T(8,128)(2,1)} %copy-done.3) | copy-start | bytes 1572868
  63.4 9.7 %copy-start.6 = (bf16[2,128,1024]{2,1,0:T(8,128)(2,1)S(1)}, bf16[2,128,1024]{2,1,0:T(8,128)(2,1)}, u32[]{:S(2)}) copy-start(bf16[2,128,1024]{2,1,0:T(8,128)(2,1)} %copy-done.5) | copy-start | bytes 1572868
  63.9 22.2 %collective-permute-start.19 = (bf16[2,128,1024]{2,1,0:T(8,128)(2,1)S(1)}, bf16[2,128,1024]{2,1,0:T(8,128)(2,1)S(1)}, u32[]{:S(2)}, u32[]{:S(2)}) collective-permute-start(bf16[2,128,1024]{2,1,0:T(8,128)(2,1)S(1)} %pad_maximum_fusion.refs_0_), channel_id=1, source_target_pairs={{0,4},{4,0},{8,12},{12,8},{16,20},{20,16},{24,28},{28,24},{1,5},{5... | collective-permute-start | bytes 1572872 | tf_op jit(solution)/shard_map/ppermute | solution.py:257
  71.5 14.6 %collective-permute-start.20 = (bf16[2,128,1024]{2,1,0:T(8,128)(2,1)S(1)}, bf16[2,128,1024]{2,1,0:T(8,128)(2,1)S(1)}, u32[]{:S(2)}, u32[]{:S(2)}) collective-permute-start(bf16[2,128,1024]{2,1,0:T(8,128)(2,1)S(1)} %collective-permute-done.4.refs_0_), channel_id=1, source_target_pairs={{0,1},{1,0},{2,3},{3,2},{4,5},{5,4},{6,7},{7,6},{8,9},{9,8},{10,11... | collective-permute-start | bytes 1572872 | tf_op jit(solution)/shard_map/ppermute | solution.py:256
  84.0 65.5 %collective-permute-start.14 = (bf16[2,384,3072]{2,1,0:T(8,128)(2,1)S(1)}, bf16[2,384,3072]{2,1,0:T(8,128)(2,1)S(1)}, u32[]{:S(2)}, u32[]{:S(2)}) collective-permute-start(bf16[2,384,3072]{2,1,0:T(8,128)(2,1)S(1)} %get-tuple-element.20.refs_1_), channel_id=1, source_target_pairs={{0,2},{2,0},{1,3},{3,1},{4,6},{6,4},{5,7},{7,5},{8,10},{10,8},{9,1... | collective-permute-start | bytes 14155784 | tf_op jit(solution)/shard_map/ppermute | solution.py:278
  84.1 14.9 %collective-permute-start.15 = (bf16[2,128,1024]{2,1,0:T(8,128)(2,1)S(1)}, bf16[2,128,1024]{2,1,0:T(8,128)(2,1)S(1)}, u32[]{:S(2)}, u32[]{:S(2)}) collective-permute-start(bf16[2,128,1024]{2,1,0:T(8,128)(2,1)S(1)} %collective-permute-done.5.refs_0_), channel_id=1, source_target_pairs={{0,1},{1,0},{2,3},{3,2},{4,5},{5,4},{6,7},{7,6},{8,9},{9,8},{10,11... | collective-permute-start | bytes 1572872 | tf_op jit(solution)/shard_map/ppermute | solution.py:256
  84.7 25.0 %collective-permute-start.16 = (bf16[2,128,1024]{2,1,0:T(8,128)(2,1)S(1)}, bf16[2,128,1024]{2,1,0:T(8,128)(2,1)S(1)}, u32[]{:S(2)}, u32[]{:S(2)}) collective-permute-start(bf16[2,128,1024]{2,1,0:T(8,128)(2,1)S(1)} %collective-permute-done.6.refs_1_), channel_id=1, source_target_pairs={{0,1},{1,0},{2,3},{3,2},{4,5},{5,4},{6,7},{7,6},{8,9},{9,8},{10,11... | collective-permute-start | bytes 1572872 | tf_op jit(solution)/shard_map/ppermute | solution.py:256
  93.8 42.8 %collective-permute-start.21 = (bf16[2,256,3072]{2,1,0:T(8,128)(2,1)S(1)}, bf16[2,256,3072]{2,1,0:T(8,128)(2,1)S(1)}, u32[]{:S(2)}, u32[]{:S(2)}) collective-permute-start(bf16[2,256,3072]{2,1,0:T(8,128)(2,1)S(1)} %get-tuple-element.26.refs_4_), channel_id=1, source_target_pairs={{0,2},{2,0},{1,3},{3,1},{4,6},{6,4},{5,7},{7,5},{8,10},{10,8},{9,1... | collective-permute-start | bytes 9437192 | tf_op jit(solution)/shard_map/ppermute | solution.py:278
  117.2 26.8 %collective-permute-start.17 = (bf16[2,256,3072]{2,1,0:T(8,128)(2,1)S(1)}, bf16[2,256,3072]{2,1,0:T(8,128)(2,1)S(1)}, u32[]{:S(2)}, u32[]{:S(2)}) collective-permute-start(bf16[2,256,3072]{2,1,0:T(8,128)(2,1)S(1)} %get-tuple-element.22.refs_1_), channel_id=1, source_target_pairs={{0,2},{2,0},{1,3},{3,1},{4,6},{6,4},{5,7},{7,5},{8,10},{10,8},{9,1... | collective-permute-start | bytes 9437192 | tf_op jit(solution)/shard_map/ppermute | solution.py:278
  127.0 9.6 %collective-permute-start.18 = (bf16[2,128,3072]{2,1,0:T(8,128)(2,1)S(1)}, bf16[2,128,3072]{2,1,0:T(8,128)(2,1)S(1)}, u32[]{:S(2)}, u32[]{:S(2)}) collective-permute-start(bf16[2,128,3072]{2,1,0:T(8,128)(2,1)S(1)} %get-tuple-element.24.refs_1_), channel_id=1, source_target_pairs={{0,2},{2,0},{1,3},{3,1},{4,6},{6,4},{5,7},{7,5},{8,10},{10,8},{9,1... | collective-permute-start | bytes 4718600 | tf_op jit(solution)/shard_map/ppermute | solution.py:278
  127.5 8.3 %collective-permute-start.3 = (bf16[128,1024]{1,0:T(8,128)(2,1)S(1)}, bf16[128,1024]{1,0:T(8,128)(2,1)S(1)}, u32[]{:S(2)}, u32[]{:S(2)}) collective-permute-start(bf16[128,1024]{1,0:T(8,128)(2,1)S(1)} %slice_bitcast_fusion), channel_id=1, source_target_pairs={{0,1},{1,0},{2,3},{3,2},{4,5},{5,4},{6,7},{7,6},{8,9},{9,8},{10,11... | collective-permute-start | bytes 786440 | tf_op jit(solution)/shard_map/ppermute | solution.py:284
where the time goes:
time: 159 us; the launch traced here: 158 us
  waiting for transfers between devices  69.4 us (44%)
  Pallas kernels  57.9 us (36%)
  starting transfers between devices  22.4 us (14%)
  local copies, waits for them, and re-layouts  5.99 us (4%)
  other arithmetic  1.85 us (1%)
    pallas_call x4, Pallas kernels, forward(): pl.pallas_call(functools.partial(forward_kernel, count, first), in_specs=...  35.7 us
    pallas_call x3, Pallas kernels, accumulate(): pl.pallas_call(functools.partial(accumulate_kernel, len(pieces), sums is...  21.7 us
    ppermute x4, waiting for transfers between devices, shards(): over.append(lax.ppermute(near[step], 'rep', across))  18 us
    ppermute x4, waiting for transfers between devices, shards(): beside.append(lax.ppermute(near[step], 'tp', swap))  15.8 us
    ppermute x3, waiting for transfers between devices, shards(): near.append(lax.ppermute(near[step], 'rep', along))  12.6 us
    ppermute x2, waiting for transfers between devices, shards(): corner[step] = lax.ppermute(corner[(step + 1) % length], 'rep', back)  8.7 us
    ppermute x1, waiting for transfers between devices, shards(): passed = lax.ppermute(partial_there, 'tp', swap)  7.69 us
    ppermute x1, waiting for transfers between devices, shards(): corner[0] = lax.ppermute(beside[0], 'rep', across)  6.65 us
  transfers between devices with their start and end apart: 22, of which 9 were waited for; matrix products, arithmetic and copies ran while one was open for 1% of the time, Pallas kernels for 31%

commit v1 on v0

--- a/solution.py
+++ b/solution.py
@@ -13,6 +13,7 @@
 SMEM = pl.BlockSpec(memory_space=pltpu.SMEM)
 HBM = pl.BlockSpec(memory_space=pltpu.HBM)
 MIB = 1 << 20
+FORWARD_MIB = 5
 
 
 def dot(left, right, contract):
@@ -51,24 +52,27 @@
 
 def forward_kernel(count, first, same_ref, *refs):
     mine, theirs = refs[:count], refs[count : 2 * count]
-    up_ref, down_ref, up_other, down_other = refs[2 * count : 2 * count + 4]
-    packet_ref, keep_ref, *part_ref = refs[2 * count + 4 : 2 * count + 6 + first]
-    give_ref, up_buf, down_buf, sems, *sum_ref = refs[2 * count + 6 + first :]
+    up_ref, down_ref, up_other, down_other, packet_ref, keep_ref, *rest = refs[2 * count :]
     _, rows, _ = mine[0].shape
-    hidden, tile = up_ref.shape[1], up_buf.shape[2]
+    hidden = up_ref.shape[1]
+    tile = tile_of(hidden)
     steps = hidden // tile
-
-    def copy(step, which):
-        slot = lax.rem(step, 2)
-        cols = pl.ds(pl.multiple_of(step * tile, tile), tile)
-        if which == 0:
-            source, target = up_other.at[:, cols], up_buf.at[slot]
-        else:
-            source, target = down_other.at[cols, :], down_buf.at[slot]
-        return pltpu.make_async_copy(source, target, sems.at[slot, which])
-
-    for which in range(2):
-        copy(0, which).start()
+    if first:
+        up_held, down_held, give_ref, sems = rest
+        sources, up_other, down_other = (up_other, down_other), up_held, down_held
+
+        def copies(step):
+            cols = pl.ds(pl.multiple_of(step * tile, tile), tile)
+            return (
+                pltpu.make_async_copy(sources[0].at[:, cols], up_held.at[:, cols], sems.at[0, step]),
+                pltpu.make_async_copy(sources[1].at[cols, :], down_held.at[cols, :], sems.at[1, step]),
+            )
+
+        for step in range(steps):
+            for copy in copies(step):
+                copy.start()
+    else:
+        (give_ref,) = rest
 
     def choose(kept, given):
         for at in range(count):
@@ -77,8 +81,6 @@
             give_ref[:, place, :] = given[at][...]
             packet_ref[:, place, hidden:] = given[at][...]
 
-    if first:
-        sum_ref[0][...] = jnp.zeros_like(sum_ref[0])
     same = same_ref[0] == 1
 
     @pl.when(same)
@@ -91,60 +93,70 @@
 
     @pl.loop(0, steps)
     def _(step):
-        slot = lax.rem(step, 2)
         cols = pl.ds(pl.multiple_of(step * tile, tile), tile)
-
-        @pl.when(step + 1 < steps)
-        def _():
-            for which in range(2):
-                copy(step + 1, which).start()
-
-        for which in range(2):
-            copy(step, which).wait()
+        if first:
+            for copy in copies(step):
+                copy.wait()
         preact = dot(keep_ref[0], up_ref[:, cols], ((1,), (0,)))
-        preact += dot(give_ref[0], up_buf[slot], ((1,), (0,)))
+        preact += dot(give_ref[0], up_other[:, cols], ((1,), (0,)))
         act_grad = dot(keep_ref[1], down_ref[cols, :], ((1,), (1,)))
-        act_grad += dot(give_ref[1], down_buf[slot], ((1,), (1,)))
+        act_grad += dot(give_ref[1], down_other[cols, :], ((1,), (1,)))
         relu_pre = jnp.maximum(preact, 0.0)
-        pre_grad = (2.0 * relu_pre * act_grad).astype(BF16)
-        packet_ref[0, :, cols] = pre_grad
+        packet_ref[0, :, cols] = (2.0 * relu_pre * act_grad).astype(BF16)
         packet_ref[1, :, cols] = (relu_pre * relu_pre).astype(BF16)
-        if first:
-            for at, held in enumerate((up_ref[:, cols], up_buf[slot])):
-                sum_ref[0][at] += dot(pre_grad[:rows], held, ((1,), (1,)))
-
-    if first:
-        part_ref[0][1 - same_ref[0]] = sum_ref[0][0].astype(BF16)
-        part_ref[0][same_ref[0]] = sum_ref[0][1].astype(BF16)
 
 
 def forward(same, mine, theirs, weights, first):
     count = len(mine)
     _, rows, part = mine[0].shape
     hidden = weights[0].shape[1]
-    tokens, tile = count * rows, tile_of(hidden)
+    tokens = count * rows
+    made = [
+        jax.ShapeDtypeStruct((2, tokens, hidden + part), BF16),
+        jax.ShapeDtypeStruct((2, tokens, part), BF16),
+    ]
+    scratch = [pltpu.VMEM((2, tokens, part), BF16)]
+    if first:
+        made += [jax.ShapeDtypeStruct(t.shape, t.dtype) for t in weights[2:]]
+        scratch += [pltpu.SemaphoreType.DMA((2, hidden // tile_of(hidden)))]
     return pl.pallas_call(
         functools.partial(forward_kernel, count, first),
-        in_specs=[SMEM] + [VMEM] * (2 * count + 2) + [HBM] * 2,
-        out_specs=[VMEM] * (2 + first),
-        out_shape=[
-            jax.ShapeDtypeStruct((2, tokens, hidden + part), BF16),
-            jax.ShapeDtypeStruct((2, tokens, part), BF16),
-            jax.ShapeDtypeStruct((2, rows, part), BF16),
-        ][: 2 + first],
-        scratch_shapes=[
-            pltpu.VMEM((2, tokens, part), BF16),
-            pltpu.VMEM((2, part, tile), BF16),
-            pltpu.VMEM((2, tile, part), BF16),
-            pltpu.SemaphoreType.DMA((2, 2)),
-            pltpu.VMEM((2, rows, part), F32),
-        ][: 4 + first],
-        compiler_params=pltpu.CompilerParams(vmem_limit_bytes=11 * MIB),
+        in_specs=[SMEM] + [VMEM] * (2 * count + 2) + [HBM if first else VMEM] * 2,
+        out_specs=[VMEM] * len(made),
+        out_shape=made,
+        scratch_shapes=scratch,
+        compiler_params=pltpu.CompilerParams(vmem_limit_bytes=FORWARD_MIB * MIB),
         cost_estimate=pl.CostEstimate(
             flops=8 * tokens * part * hidden, bytes_accessed=8 * part * hidden, transcendentals=0
         ),
         name="forward",
     )(same, *mine, *theirs, *weights)
+
+
+def inputs_kernel(same_ref, packet_ref, up_ref, up_other, out_ref):
+    _, rows, part = out_ref.shape
+    tile = tile_of(part)
+    pre_grad = packet_ref[0, :rows, : up_ref.shape[1]]
+    same = same_ref[0]
+    for held, here in ((up_ref, 1 - same), (up_other, same)):
+        for at in range(0, part, tile):
+            place = pl.ds(at, tile)
+            out_ref[here, :, place] = dot(pre_grad, held[place, :], ((1,), (1,))).astype(BF16)
+
+
+def inputs_part(same, packet, rows, held_up, other_up):
+    part, hidden = held_up.shape
+    return pl.pallas_call(
+        inputs_kernel,
+        in_specs=[SMEM] + [VMEM] * 3,
+        out_specs=VMEM,
+        out_shape=jax.ShapeDtypeStruct((2, rows, part), BF16),
+        compiler_params=pltpu.CompilerParams(vmem_limit_bytes=FORWARD_MIB * MIB),
+        cost_estimate=pl.CostEstimate(
+            flops=4 * rows * part * hidden, bytes_accessed=4 * part * hidden, transcendentals=0
+        ),
+        name="inputs_part",
+    )(same, packet, held_up, other_up)
 
 
 def grads_of(pieces, cols, hidden):
@@ -160,8 +172,7 @@
             parts += [keep[which], got[which, :, hidden:]]
         return jnp.concatenate(parts, axis=0)
 
-    up = dot(tokens(0), rows(0), ((0,), (0,)))
-    return up, dot(rows(1), tokens(1), ((0,), (0,)))
+    return lambda: dot(tokens(0), rows(0), ((0,), (0,))), lambda: dot(rows(1), tokens(1), ((0,), (0,)))
 
 
 def triples(refs, count):
@@ -178,10 +189,10 @@
     def add(step, up_to, down_to):
         cols = pl.ds(pl.multiple_of(step * tile, tile), tile)
         up, down = grads_of(pieces, cols, hidden)
-        if not first:
-            up, down = up_in[:, cols].astype(F32) + up, down_in[cols, :].astype(F32) + down
-        up_ref[:, up_to(cols)] = up.astype(up_ref.dtype)
-        down_ref[down_to(cols), :] = down.astype(down_ref.dtype)
+        total = up() if first else up_in[:, cols].astype(F32) + up()
+        up_ref[:, up_to(cols)] = total.astype(up_ref.dtype)
+        total = down() if first else down_in[cols, :].astype(F32) + down()
+        down_ref[down_to(cols), :] = total.astype(down_ref.dtype)
 
     if last:
         add(pl.program_id(0), lambda cols: slice(None), lambda cols: slice(None))
@@ -203,7 +214,7 @@
             jax.ShapeDtypeStruct((part, hidden), F32 if last else BF16),
             jax.ShapeDtypeStruct((hidden, part), F32 if last else BF16),
         ],
-        compiler_params=pltpu.CompilerParams(vmem_limit_bytes=(16 if last else 9) * MIB),
+        compiler_params=pltpu.CompilerParams(vmem_limit_bytes=(12 if last else 7) * MIB),
         cost_estimate=pl.CostEstimate(
             flops=8 * tokens * part * hidden, bytes_accessed=8 * part * hidden, transcendentals=0
         ),
@@ -246,23 +257,25 @@
         same = lax.axis_index("fs") == lax.axis_index("tp")
         flag = same.astype(jnp.int32)[None]
 
-        near = [jnp.stack([inputs, cotangent])]
-        beside, over, corner = [], [], {}
+        far_end = length - 1 if length > 2 else None
+        near = {0: jnp.stack([inputs, cotangent])}
+        beside = {0: lax.ppermute(near[0], "tp", swap)}
+        over = {0: lax.ppermute(near[0], "rep", across)}
+        corner = {0: lax.ppermute(beside[0], "rep", across)}
+        for step in range(1, length):
+            near[step] = lax.ppermute(near[step - 1], "rep", along)
+            if step == far_end:
+                beside[step] = lax.ppermute(beside[0], "rep", back)
+                over[step] = lax.ppermute(over[0], "rep", back)
+                corner[step] = lax.ppermute(beside[step], "rep", across)
+            else:
+                beside[step] = lax.ppermute(near[step], "tp", swap)
+                over[step] = lax.ppermute(near[step], "rep", across)
+                corner[step] = lax.ppermute(over[step], "tp", swap)
         other_up = lax.ppermute(w_up, "fs", swap)
         other_down = lax.ppermute(w_down, "fs", swap)
         weights = (w_up, w_down, other_up, other_down)
         flag = ready(flag, w_up, w_down)
-        for step in range(length):
-            beside.append(lax.ppermute(near[step], "tp", swap))
-            over.append(lax.ppermute(near[step], "rep", across))
-            if step == 0:
-                corner[0] = lax.ppermute(beside[0], "rep", across)
-            if step + 1 < length:
-                near.append(lax.ppermute(near[step], "rep", along))
-        for step in range(length - 1, 1, -1):
-            corner[step] = lax.ppermute(corner[(step + 1) % length], "rep", back)
-        if length > 1:
-            corner[1] = lax.ppermute(over[1], "tp", swap)
         own = [(near[k], beside[k]) for k in range(length)]
         far = [(over[k], corner[k]) for k in range(length)]
         groups = {f"o{k}": group for k, group in enumerate(own)}
@@ -270,19 +283,20 @@
 
         made = []
         for at, names in enumerate(CHUNKS):
-            packet, keep, *partial_value = forward(
+            packet, keep, *more = forward(
                 flag, *zip(*(groups[name] for name in names)), weights, at == 0
             )
             if at == 0:
-                partial_here, partial_there = partial_value[0]
+                weights = (w_up, w_down, *more)
             made.append((keep, packet, lax.ppermute(packet, "fs", swap)))
         sums = None
         for at, chunks in enumerate(BATCHES):
             sums = accumulate([made[k] for k in chunks], sums, at == len(BATCHES) - 1)
         grad_up, grad_down = sums
 
-        passed = lax.ppermute(partial_there, "tp", swap)
-        grad_inputs = (partial_here.astype(F32) + passed.astype(F32)).astype(BF16)
+        partial_value = inputs_part(flag, made[0][1], rows, w_up, weights[2])
+        passed = lax.ppermute(partial_value[1], "tp", swap)
+        grad_inputs = (partial_value[0].astype(F32) + passed.astype(F32)).astype(BF16)
         if n_rep > group:
             sets = [[base * group + at for base in range(n_rep // group)] for at in range(group)]
             grad_up, grad_down = (
@@ -293,7 +307,7 @@
     return shards
 
 
-CHUNKS = (("o0",), ("o1", "f0"), ("o2", "o3"), ("f3", "f1", "f2"))
+CHUNKS = (("o0",), ("o1", "f0"), ("o2", "f1", "o3"), ("f2", "f3"))
 BATCHES = ((0, 1), (2,), (3,))
 
 

time: 159 us -> 169 us (1.063)
  starting transfers between devices: 22.4 us -> 31.1 us
  local copies, waits for them, and re-layouts: 5.99 us -> 11.5 us
  Pallas kernels: 57.9 us -> 53.9 us
    ppermute x16, starting transfers between devices: 21 us -> 29.7 us  [the longest x3 16.9 us: shards(): near[step] = lax.ppermute(near[step - 1], 'rep', along)]
    pallas_call x4, Pallas kernels: 35.7 us -> 28 us  [forward(): pl.pallas_call(functools.partial(forward_kernel, count, first), in_specs=...]
    unnamed x14 -> x12, local copies, waits for them, and re-layouts: 5.97 us -> 11.5 us
    pallas_call x0 -> x1, Pallas kernels: none -> 3.49 us  [inputs_part(): pl.pallas_call(inputs_kernel, in_specs=[SMEM] + [VMEM] * 3, out_specs=VME...]
  transfers between devices with their start and end apart: 22 -> 22, of which waited for: 9 -> 9; matrix products, arithmetic and copies ran while one was open for 1% -> 1% of each run, Pallas kernels for 31% -> 22%
where the time goes in v1:
time: 169 us
  waiting for transfers between devices  69.7 us (41%)
  Pallas kernels  53.9 us (32%)
  starting transfers between devices  31.1 us (18%)
  local copies, waits for them, and re-layouts  11.5 us (7%)
  other arithmetic  1.85 us (1%)
    pallas_call x4, Pallas kernels, forward(): pl.pallas_call(functools.partial(forward_kernel, count, first), in_specs=...  28 us
    pallas_call x3, Pallas kernels, accumulate(): pl.pallas_call(functools.partial(accumulate_kernel, len(pieces), sums is...  21.9 us
    ppermute x3, starting transfers between devices, shards(): near[step] = lax.ppermute(near[step - 1], 'rep', along)  16.9 us
    ppermute x2, waiting for transfers between devices, shards(): over[step] = lax.ppermute(near[step], 'rep', across)  13.4 us
    ppermute x3, waiting for transfers between devices, shards(): near[step] = lax.ppermute(near[step - 1], 'rep', along)  13.2 us
    ppermute x1, waiting for transfers between devices, shards(): over = {0: lax.ppermute(near[0], 'rep', across)}  11.7 us
    unnamed x12, local copies, waits for them, and re-layouts  11.5 us
    ppermute x1, waiting for transfers between devices, shards(): corner = {0: lax.ppermute(beside[0], 'rep', across)}  11.2 us
  transfers between devices with their start and end apart: 22, of which 9 were waited for; matrix products, arithmetic and copies ran while one was open for 1% of the time, Pallas kernels for 22%

profile of v1, /device:TPU:0, one launch (start us, length us, event | category | flops | bytes accessed | tf_op | source)
XLA Modules:
  0.0 168.8 jit_solution(5733817914822173044)
XLA Ops:
  1.3 1.1 pad_maximum_fusion.refs_0_
  2.4 3.0 %collective-permute-start.4 = (bf16[2,128,1024]{2,1,0:T(8,128)(2,1)S(1)}, bf16[2,128,1024]{2,1,0:T(8,128)(2,1)S(1)}, u32[]{:S(2)}, u32[]{:S(2)}) collective-permute-start(bf16[2,128,1024]{2,1,0:T(8,128)(2,1)S(1)} %pad_maximum_fusion.refs_0_), channel_id=1, source_target_pairs={{0,8},{4,12},{8,24},{12,28},{16,0},{20,4},{24,16},{28,20},{1,9},{5... | collective-permute-start | bytes 1572872 | tf_op jit(solution)/shard_map/ppermute | solution.py:266
  5.4 1.5 collective-permute-start
  6.9 11.7 %collective-permute-done.4.refs_0_ = bf16[2,128,1024]{2,1,0:T(8,128)(2,1)S(1)} collective-permute-done((bf16[2,128,1024]{2,1,0:T(8,128)(2,1)S(1)}, bf16[2,128,1024]{2,1,0:T(8,128)(2,1)S(1)}, u32[]{:S(2)}, u32[]{:S(2)}) %collective-permute-start.4) | collective-permute-done | bytes 524320 | tf_op jit(solution)/shard_map/ppermute | solution.py:266
  18.6 1.6 collective-permute-start.13
  20.9 2.1 %collective-permute-start.10 = (bf16[2,128,1024]{2,1,0:T(8,128)(2,1)S(1)}, bf16[2,128,1024]{2,1,0:T(8,128)(2,1)S(1)}, u32[]{:S(2)}, u32[]{:S(2)}) collective-permute-start(bf16[2,128,1024]{2,1,0:T(8,128)(2,1)S(1)} %collective-permute-done.refs_1_), channel_id=1, source_target_pairs={{8,0},{12,4},{24,8},{28,12},{0,16},{4,20},{16,24},{20,28},{9,1},{1... | collective-permute-start | bytes 1572872 | tf_op jit(solution)/shard_map/ppermute | solution.py:268
  23.1 8.8 %collective-permute-done.13.refs_1_ = bf16[2,128,1024]{2,1,0:T(8,128)(2,1)S(1)} collective-permute-done((bf16[2,128,1024]{2,1,0:T(8,128)(2,1)S(1)}, bf16[2,128,1024]{2,1,0:T(8,128)(2,1)S(1)}, u32[]{:S(2)}, u32[]{:S(2)}) %collective-permute-start.13) | collective-permute-done | bytes 524320 | tf_op jit(solution)/shard_map/ppermute | solution.py:273
  31.9 1.3 collective-permute-start.16
  33.2 1.5 collective-permute-done.5.refs_0_
  34.7 1.5 collective-permute-start.15
  36.2 2.0 %copy-done.4 = bf16[2048,1024]{1,0:T(8,128)(2,1)} copy-done((bf16[2048,1024]{1,0:T(8,128)(2,1)}, bf16[2048,1024]{1,0:T(8,128)(2,1)S(1)}, u32[]{:S(2)}) %copy-start.4) | copy-done | bytes 4194328
  38.2 13.1 %collective-permute-start.14 = (bf16[2,128,1024]{2,1,0:T(8,128)(2,1)S(1)}, bf16[2,128,1024]{2,1,0:T(8,128)(2,1)}, u32[]{:S(2)}, u32[]{:S(2)}) collective-permute-start(bf16[2,128,1024]{2,1,0:T(8,128)(2,1)S(1)} %collective-permute-done.5.refs_0_), channel_id=1, source_target_pairs={{0,8},{4,12},{8,24},{12,28},{16,0},{20,4},{24,16},{28,20},{1,9},{5... | collective-permute-start | bytes 1572872 | tf_op jit(solution)/shard_map/ppermute | solution.py:266
  51.3 2.2 %copy-done = bf16[1024,2048]{1,0:T(8,128)(2,1)S(1)} copy-done((bf16[1024,2048]{1,0:T(8,128)(2,1)S(1)}, bf16[1024,2048]{1,0:T(8,128)(2,1)}, u32[]{:S(2)}) %copy-start) | copy-done | bytes 4194328
  53.4 2.2 %copy-done.2 = bf16[2048,1024]{1,0:T(8,128)(2,1)S(1)} copy-done((bf16[2048,1024]{1,0:T(8,128)(2,1)S(1)}, bf16[2048,1024]{1,0:T(8,128)(2,1)}, u32[]{:S(2)}) %copy-start.2) | copy-done | bytes 4194328
  56.2 1.6 copy-done.1
  57.8 1.3 copy-done.3
  59.1 2.2 %copy-done.5 = bf16[2048,1024]{1,0:T(8,128)(2,1)S(1)} copy-done((bf16[2048,1024]{1,0:T(8,128)(2,1)S(1)}, bf16[2048,1024]{1,0:T(8,128)(2,1)}, u32[]{:S(2)}) %copy-start.5) | copy-done | bytes 4194328
  61.3 6.5 %forward.4 = (bf16[2,128,3072]{2,1,0:T(8,128)(2,1)S(1)}, bf16[2,128,1024]{2,1,0:T(8,128)(2,1)S(1)}, bf16[1024,2048]{1,0:T(8,128)(2,1)S(1)}, bf16[2048,1024]{1,0:T(8,128)(2,1)S(1)}) custom-call(s32[1]{0:T(128)} %ready.1.same_ref, bf16[2,128,1024]{2,1,0:T(8,128)(2,1)S(1)} %pad_maximum_fusion.refs_0_, bf16[2,128,1024]{2,1,0:T(8,128)(2,1)S(1)} %collective-permute-done.refs_1_, ...), custom_call_target="tpu_custom_call" | custom-call | flops 2147483648 | bytes 16777216 | tf_op jit(solution)/shard_map/forward/pallas_call | solution.py:122
  67.8 9.5 %forward.6 = (bf16[2,384,3072]{2,1,0:T(8,128)(2,1)S(1)}, bf16[2,384,1024]{2,1,0:T(8,128)(2,1)S(1)}) custom-call(s32[1]{0:T(128)} %ready.1.same_ref, bf16[2,128,1024]{2,1,0:T(8,128)(2,1)S(1)} %collective-permute-done.5.refs_0_, bf16[2,128,1024]{2,1,0:T(8,128)(2,1)S(1)} %collective-permute-done.13.refs_1_, ...), custom_call_target="tpu_custom_call" | custom-call | flops 6442450944 | bytes 16777216 | tf_op jit(solution)/shard_map/forward/pallas_call | solution.py:122
  78.5 1.5 collective-permute-start.20
  80.6 11.7 %collective-permute-done.7.refs_1_ = bf16[2,128,1024]{2,1,0:T(8,128)(2,1)S(1)} collective-permute-done((bf16[2,128,1024]{2,1,0:T(8,128)(2,1)S(1)}, bf16[2,128,1024]{2,1,0:T(8,128)(2,1)S(1)}, u32[]{:S(2)}, u32[]{:S(2)}) %collective-permute-start.7) | collective-permute-done | bytes 524320 | tf_op jit(solution)/shard_map/ppermute | solution.py:263
  92.3 11.2 %collective-permute-done.20.refs_3_ = bf16[2,128,1024]{2,1,0:T(8,128)(2,1)S(1)} collective-permute-done((bf16[2,128,1024]{2,1,0:T(8,128)(2,1)S(1)}, bf16[2,128,1024]{2,1,0:T(8,128)(2,1)S(1)}, u32[]{:S(2)}, u32[]{:S(2)}) %collective-permute-start.20) | collective-permute-done | bytes 524320 | tf_op jit(solution)/shard_map/ppermute | solution.py:264
  103.5 5.9 %forward.7 = (bf16[2,256,3072]{2,1,0:T(8,128)(2,1)S(1)}, bf16[2,256,1024]{2,1,0:T(8,128)(2,1)S(1)}) custom-call(s32[1]{0:T(128)} %ready.1.same_ref, bf16[2,128,1024]{2,1,0:T(8,128)(2,1)S(1)} %collective-permute-done.4.refs_0_, bf16[2,128,1024]{2,1,0:T(8,128)(2,1)S(1)} %collective-permute-done.7.refs_1_, ...), custom_call_target="tpu_custom_call" | custom-call | flops 4294967296 | bytes 16777216 | tf_op jit(solution)/shard_map/forward/pallas_call | solution.py:122
  110.1 4.6 %collective-permute-done.6.refs_0_ = bf16[2,128,1024]{2,1,0:T(8,128)(2,1)S(1)} collective-permute-done((bf16[2,128,1024]{2,1,0:T(8,128)(2,1)S(1)}, bf16[2,128,1024]{2,1,0:T(8,128)(2,1)S(1)}, u32[]{:S(2)}, u32[]{:S(2)}) %collective-permute-start.6) | collective-permute-done | bytes 524320 | tf_op jit(solution)/shard_map/ppermute | solution.py:273
  115.3 10.2 %collective-permute-done.8.refs_1_ = bf16[2,128,1024]{2,1,0:T(8,128)(2,1)S(1)} collective-permute-done((bf16[2,128,1024]{2,1,0:T(8,128)(2,1)S(1)}, bf16[2,128,1024]{2,1,0:T(8,128)(2,1)S(1)}, u32[]{:S(2)}, u32[]{:S(2)}) %collective-permute-start.8) | collective-permute-done | bytes 524320 | tf_op jit(solution)/shard_map/ppermute | solution.py:269
  125.5 2.1 %collective-permute-done.9.refs_2_ = bf16[2,128,1024]{2,1,0:T(8,128)(2,1)S(1)} collective-permute-done((bf16[2,128,1024]{2,1,0:T(8,128)(2,1)S(1)}, bf16[2,128,1024]{2,1,0:T(8,128)(2,1)S(1)}, u32[]{:S(2)}, u32[]{:S(2)}) %collective-permute-start.9) | collective-permute-done | bytes 524320 | tf_op jit(solution)/shard_map/ppermute | solution.py:274
  127.6 6.1 %forward.5 = (bf16[2,256,3072]{2,1,0:T(8,128)(2,1)S(1)}, bf16[2,256,1024]{2,1,0:T(8,128)(2,1)S(1)}) custom-call(s32[1]{0:T(128)} %ready.1.same_ref, bf16[2,128,1024]{2,1,0:T(8,128)(2,1)S(1)} %collective-permute-done.6.refs_0_, bf16[2,128,1024]{2,1,0:T(8,128)(2,1)S(1)} %collective-permute-done.8.refs_1_, ...), custom_call_target="tpu_custom_call" | custom-call | flops 4294967296 | bytes 16777216 | tf_op jit(solution)/shard_map/forward/pallas_call | solution.py:122
  134.3 3.5 %inputs_part.1 = bf16[2,128,1024]{2,1,0:T(8,128)(2,1)S(1)} custom-call(s32[1]{0:T(128)} %ready.1.same_ref, bf16[2,128,3072]{2,1,0:T(8,128)(2,1)S(1)} %get-tuple-element.19.packet_ref.refs_1_, bf16[1024,2048]{1,0:T(8,128)(2,1)S(1)} %copy-done.1, bf16[1024,2048]{1,0:T(8,128)(2,1)S(1)} %get-tuple-element.20.up_other.refs_6_.refs_8_), custom_call_target="tpu_custom_call" | custom-call | flops 1073741824 | bytes 8388608 | tf_op jit(solution)/shard_map/inputs_part/pallas_call | solution.py:149
  138.4 7.8 %collective-permute-done.3 = bf16[128,1024]{1,0:T(8,128)(2,1)S(1)} collective-permute-done((bf16[128,1024]{1,0:T(8,128)(2,1)S(1)}, bf16[128,1024]{1,0:T(8,128)(2,1)S(1)}, u32[]{:S(2)}, u32[]{:S(2)}) %collective-permute-start.3) | collective-permute-done | bytes 262176 | tf_op jit(solution)/shard_map/ppermute | solution.py:298
  146.9 7.4 %accumulate.3 = (bf16[1024,2048]{1,0:T(8,128)(2,1)S(1)}, bf16[2048,1024]{1,0:T(8,128)(2,1)S(1)}) custom-call(bf16[2,128,1024]{2,1,0:T(8,128)(2,1)S(1)} %get-tuple-element.26.refs_0_, bf16[2,128,3072]{2,1,0:T(8,128)(2,1)S(1)} %get-tuple-element.19.packet_ref.refs_1_, bf16[2,128,3072]{2,1,0:T(8,128)(2,1)S(1)} %collective-permute-done.18.refs_2_, ...), custom_call_target="tpu_custom_call" | custom-call | flops 6442450944 | bytes 16777216 | tf_op jit(solution)/shard_map/accumulate/pallas_call | solution.py:233
  154.4 7.6 %accumulate.4 = (bf16[1024,2048]{1,0:T(8,128)(2,1)S(1)}, bf16[2048,1024]{1,0:T(8,128)(2,1)S(1)}) custom-call(bf16[2,384,1024]{2,1,0:T(8,128)(2,1)S(1)} %get-tuple-element.24.refs_0_, bf16[2,384,3072]{2,1,0:T(8,128)(2,1)S(1)} %get-tuple-element.25.refs_1_, ...), custom_call_target="tpu_custom_call", output_to_operand_aliasing={{0}: (3, {}), {1}: (4, {})} | custom-call | flops 6442450944 | bytes 16777216 | tf_op jit(solution)/shard_map/accumulate/pallas_call | solution.py:233
  162.0 6.8 %accumulate.5 = (f32[1024,2048]{1,0:T(8,128)}, f32[2048,1024]{1,0:T(8,128)}) custom-call(bf16[2,256,1024]{2,1,0:T(8,128)(2,1)S(1)} %get-tuple-element.22.refs_0_, bf16[2,256,3072]{2,1,0:T(8,128)(2,1)S(1)} %get-tuple-element.23.refs_1_, bf16[2,256,3072]{2,1,0:T(8,128)(2,1)S(1)} %collective-permute-done.12.refs_2_, ...), custom_call_target="tpu_custom_call" | custom-call | flops 4294967296 | bytes 16777216 | tf_op jit(solution)/shard_map/accumulate/pallas_call | solution.py:233
  (36 shorter events, 6.9 us)
Async XLA Ops:
  0.6 35.5 %collective-permute-start.2 = (bf16[2048,1024]{1,0:T(8,128)(2,1)}, bf16[2048,1024]{1,0:T(8,128)(2,1)S(1)}, u32[]{:S(2)}, u32[]{:S(2)}) collective-permute-start(bf16[2048,1024]{1,0:T(8,128)(2,1)} %refs_5_.3), channel_id=1, source_target_pairs={{0,2},{2,0},{1,3},{3,1},{4,6},{6,4},{5,7},{7,5},{8,10},{10,8},{9,1... | collective-permute-start | bytes 12582920 | tf_op jit(solution)/shard_map/ppermute | solution.py:276
  1.2 55.0 %collective-permute-start.1 = (bf16[1024,2048]{1,0:T(8,128)(2,1)}, bf16[1024,2048]{1,0:T(8,128)(2,1)}, u32[]{:S(2)}, u32[]{:S(2)}) collective-permute-start(bf16[1024,2048]{1,0:T(8,128)(2,1)} %refs_4_.3), channel_id=1, source_target_pairs={{0,2},{2,0},{1,3},{3,1},{4,6},{6,4},{5,7},{7,5},{8,10},{10,8},{9,1... | collective-permute-start | bytes 12582920 | tf_op jit(solution)/shard_map/ppermute | solution.py:275
  2.4 16.2 %collective-permute-start.4 = (bf16[2,128,1024]{2,1,0:T(8,128)(2,1)S(1)}, bf16[2,128,1024]{2,1,0:T(8,128)(2,1)S(1)}, u32[]{:S(2)}, u32[]{:S(2)}) collective-permute-start(bf16[2,128,1024]{2,1,0:T(8,128)(2,1)S(1)} %pad_maximum_fusion.refs_0_), channel_id=1, source_target_pairs={{0,8},{4,12},{8,24},{12,28},{16,0},{20,4},{24,16},{28,20},{1,9},{5... | collective-permute-start | bytes 1572872 | tf_op jit(solution)/shard_map/ppermute | solution.py:266
  5.4 15.5 %collective-permute-start = (bf16[2,128,1024]{2,1,0:T(8,128)(2,1)S(1)}, bf16[2,128,1024]{2,1,0:T(8,128)(2,1)S(1)}, u32[]{:S(2)}, u32[]{:S(2)}) collective-permute-start(bf16[2,128,1024]{2,1,0:T(8,128)(2,1)S(1)} %pad_maximum_fusion.refs_0_), channel_id=1, source_target_pairs={{0,1},{1,0},{2,3},{3,2},{4,5},{5,4},{6,7},{7,6},{8,9},{9,8},{10,11... | collective-permute-start | bytes 1572872 | tf_op jit(solution)/shard_map/ppermute | solution.py:262
  18.6 13.3 %collective-permute-start.13 = (bf16[2,128,1024]{2,1,0:T(8,128)(2,1)S(1)}, bf16[2,128,1024]{2,1,0:T(8,128)(2,1)S(1)}, u32[]{:S(2)}, u32[]{:S(2)}) collective-permute-start(bf16[2,128,1024]{2,1,0:T(8,128)(2,1)S(1)} %collective-permute-done.4.refs_0_), channel_id=1, source_target_pairs={{0,4},{4,0},{8,12},{12,8},{16,20},{20,16},{24,28},{28,24},{1,5},{5... | collective-permute-start | bytes 1572872 | tf_op jit(solution)/shard_map/ppermute | solution.py:273
  20.1 14.5 %collective-permute-start.5 = (bf16[2,128,1024]{2,1,0:T(8,128)(2,1)S(1)}, bf16[2,128,1024]{2,1,0:T(8,128)(2,1)S(1)}, u32[]{:S(2)}, u32[]{:S(2)}) collective-permute-start(bf16[2,128,1024]{2,1,0:T(8,128)(2,1)S(1)} %collective-permute-done.4.refs_0_), channel_id=1, source_target_pairs={{0,8},{4,12},{8,24},{12,28},{16,0},{20,4},{24,16},{28,20},{1,9},{5... | collective-permute-start | bytes 1572872 | tf_op jit(solution)/shard_map/ppermute | solution.py:266
  20.9 46.8 %collective-permute-start.10 = (bf16[2,128,1024]{2,1,0:T(8,128)(2,1)S(1)}, bf16[2,128,1024]{2,1,0:T(8,128)(2,1)S(1)}, u32[]{:S(2)}, u32[]{:S(2)}) collective-permute-start(bf16[2,128,1024]{2,1,0:T(8,128)(2,1)S(1)} %collective-permute-done.refs_1_), channel_id=1, source_target_pairs={{8,0},{12,4},{24,8},{28,12},{0,16},{4,20},{16,24},{20,28},{9,1},{1... | collective-permute-start | bytes 1572872 | tf_op jit(solution)/shard_map/ppermute | solution.py:268
  31.9 35.9 %collective-permute-start.16 = (bf16[2,128,1024]{2,1,0:T(8,128)(2,1)S(1)}, bf16[2,128,1024]{2,1,0:T(8,128)(2,1)}, u32[]{:S(2)}, u32[]{:S(2)}) collective-permute-start(bf16[2,128,1024]{2,1,0:T(8,128)(2,1)S(1)} %collective-permute-done.13.refs_1_), channel_id=1, source_target_pairs={{0,1},{1,0},{2,3},{3,2},{4,5},{5,4},{6,7},{7,6},{8,9},{9,8},{10,11... | collective-permute-start | bytes 1572872 | tf_op jit(solution)/shard_map/ppermute | solution.py:274
  34.7 33.1 %collective-permute-start.15 = (bf16[2,128,1024]{2,1,0:T(8,128)(2,1)S(1)}, bf16[2,128,1024]{2,1,0:T(8,128)(2,1)}, u32[]{:S(2)}, u32[]{:S(2)}) collective-permute-start(bf16[2,128,1024]{2,1,0:T(8,128)(2,1)S(1)} %collective-permute-done.5.refs_0_), channel_id=1, source_target_pairs={{0,1},{1,0},{2,3},{3,2},{4,5},{5,4},{6,7},{7,6},{8,9},{9,8},{10,11... | collective-permute-start | bytes 1572872 | tf_op jit(solution)/shard_map/ppermute | solution.py:272
  36.2 2.0 %copy-start.4 = (bf16[2048,1024]{1,0:T(8,128)(2,1)}, bf16[2048,1024]{1,0:T(8,128)(2,1)S(1)}, u32[]{:S(2)}) copy-start(bf16[2048,1024]{1,0:T(8,128)(2,1)S(1)} %collective-permute-done.2.refs_5_) | copy-start | bytes 12582916
  38.2 29.6 %collective-permute-start.14 = (bf16[2,128,1024]{2,1,0:T(8,128)(2,1)S(1)}, bf16[2,128,1024]{2,1,0:T(8,128)(2,1)}, u32[]{:S(2)}, u32[]{:S(2)}) collective-permute-start(bf16[2,128,1024]{2,1,0:T(8,128)(2,1)S(1)} %collective-permute-done.5.refs_0_), channel_id=1, source_target_pairs={{0,8},{4,12},{8,24},{12,28},{16,0},{20,4},{24,16},{28,20},{1,9},{5... | collective-permute-start | bytes 1572872 | tf_op jit(solution)/shard_map/ppermute | solution.py:266
  51.2 2.2 %copy-start = (bf16[1024,2048]{1,0:T(8,128)(2,1)S(1)}, bf16[1024,2048]{1,0:T(8,128)(2,1)}, u32[]{:S(2)}) copy-start(bf16[1024,2048]{1,0:T(8,128)(2,1)} %refs_4_.3) | copy-start | bytes 12582916
  53.4 2.2 %copy-start.2 = (bf16[2048,1024]{1,0:T(8,128)(2,1)S(1)}, bf16[2048,1024]{1,0:T(8,128)(2,1)}, u32[]{:S(2)}) copy-start(bf16[2048,1024]{1,0:T(8,128)(2,1)} %refs_5_.3) | copy-start | bytes 12582916
  55.6 2.2 %copy-start.1 = (bf16[1024,2048]{1,0:T(8,128)(2,1)S(1)}, bf16[1024,2048]{1,0:T(8,128)(2,1)}, u32[]{:S(2)}) copy-start(bf16[1024,2048]{1,0:T(8,128)(2,1)} %refs_4_.3) | copy-start | bytes 12582916
  55.6 3.5 %copy-start.3 = (bf16[2048,1024]{1,0:T(8,128)(2,1)S(1)}, bf16[2048,1024]{1,0:T(8,128)(2,1)}, u32[]{:S(2)}) copy-start(bf16[2048,1024]{1,0:T(8,128)(2,1)} %refs_5_.3) | copy-start | bytes 12582916
  59.1 2.2 %copy-start.5 = (bf16[2048,1024]{1,0:T(8,128)(2,1)S(1)}, bf16[2048,1024]{1,0:T(8,128)(2,1)}, u32[]{:S(2)}) copy-start(bf16[2048,1024]{1,0:T(8,128)(2,1)} %copy-done.4) | copy-start | bytes 12582916
  77.3 77.0 %collective-permute-start.17 = (bf16[2,384,3072]{2,1,0:T(8,128)(2,1)S(1)}, bf16[2,384,3072]{2,1,0:T(8,128)(2,1)S(1)}, u32[]{:S(2)}, u32[]{:S(2)}) collective-permute-start(bf16[2,384,3072]{2,1,0:T(8,128)(2,1)S(1)} %get-tuple-element.25.refs_1_), channel_id=1, source_target_pairs={{0,2},{2,0},{1,3},{3,1},{4,6},{6,4},{5,7},{7,5},{8,10},{10,8},{9,1... | collective-permute-start | bytes 14155784 | tf_op jit(solution)/shard_map/ppermute | solution.py:291
  77.4 14.9 %collective-permute-start.7 = (bf16[2,128,1024]{2,1,0:T(8,128)(2,1)S(1)}, bf16[2,128,1024]{2,1,0:T(8,128)(2,1)S(1)}, u32[]{:S(2)}, u32[]{:S(2)}) collective-permute-start(bf16[2,128,1024]{2,1,0:T(8,128)(2,1)S(1)} %pad_maximum_fusion.refs_0_), channel_id=1, source_target_pairs={{0,4},{4,0},{8,12},{12,8},{16,20},{20,16},{24,28},{28,24},{1,5},{5... | collective-permute-start | bytes 1572872 | tf_op jit(solution)/shard_map/ppermute | solution.py:263
  78.0 14.3 %collective-permute-start.19 = (bf16[2,128,1024]{2,1,0:T(8,128)(2,1)S(1)}, bf16[2,128,1024]{2,1,0:T(8,128)(2,1)S(1)}, u32[]{:S(2)}, u32[]{:S(2)}) collective-permute-start(bf16[2,128,1024]{2,1,0:T(8,128)(2,1)S(1)} %collective-permute-done.4.refs_0_), channel_id=1, source_target_pairs={{0,1},{1,0},{2,3},{3,2},{4,5},{5,4},{6,7},{7,6},{8,9},{9,8},{10,11... | collective-permute-start | bytes 1572872 | tf_op jit(solution)/shard_map/ppermute | solution.py:272
  78.5 25.0 %collective-permute-start.20 = (bf16[2,128,1024]{2,1,0:T(8,128)(2,1)S(1)}, bf16[2,128,1024]{2,1,0:T(8,128)(2,1)S(1)}, u32[]{:S(2)}, u32[]{:S(2)}) collective-permute-start(bf16[2,128,1024]{2,1,0:T(8,128)(2,1)S(1)} %collective-permute-done.refs_1_), channel_id=1, source_target_pairs={{0,4},{4,0},{8,12},{12,8},{16,20},{20,16},{24,28},{28,24},{1,5},{5... | collective-permute-start | bytes 1572872 | tf_op jit(solution)/shard_map/ppermute | solution.py:264
  80.0 34.7 %collective-permute-start.6 = (bf16[2,128,1024]{2,1,0:T(8,128)(2,1)S(1)}, bf16[2,128,1024]{2,1,0:T(8,128)(2,1)S(1)}, u32[]{:S(2)}, u32[]{:S(2)}) collective-permute-start(bf16[2,128,1024]{2,1,0:T(8,128)(2,1)S(1)} %collective-permute-done.5.refs_0_), channel_id=1, source_target_pairs={{0,4},{4,0},{8,12},{12,8},{16,20},{20,16},{24,28},{28,24},{1,5},{5... | collective-permute-start | bytes 1572872 | tf_op jit(solution)/shard_map/ppermute | solution.py:273
  109.4 37.5 %collective-permute-start.21 = (bf16[2,256,3072]{2,1,0:T(8,128)(2,1)S(1)}, bf16[2,256,3072]{2,1,0:T(8,128)(2,1)S(1)}, u32[]{:S(2)}, u32[]{:S(2)}) collective-permute-start(bf16[2,256,3072]{2,1,0:T(8,128)(2,1)S(1)} %get-tuple-element.28.refs_4_), channel_id=1, source_target_pairs={{0,2},{2,0},{1,3},{3,1},{4,6},{6,4},{5,7},{7,5},{8,10},{10,8},{9,1... | collective-permute-start | bytes 9437192 | tf_op jit(solution)/shard_map/ppermute | solution.py:291
  109.5 16.0 %collective-permute-start.8 = (bf16[2,128,1024]{2,1,0:T(8,128)(2,1)S(1)}, bf16[2,128,1024]{2,1,0:T(8,128)(2,1)S(1)}, u32[]{:S(2)}, u32[]{:S(2)}) collective-permute-start(bf16[2,128,1024]{2,1,0:T(8,128)(2,1)S(1)} %collective-permute-done.7.refs_1_), channel_id=1, source_target_pairs={{8,0},{12,4},{24,8},{28,12},{0,16},{4,20},{16,24},{20,28},{9,1},{1... | collective-permute-start | bytes 1572872 | tf_op jit(solution)/shard_map/ppermute | solution.py:269
  109.6 15.9 %collective-permute-start.11 = (bf16[2,128,1024]{2,1,0:T(8,128)(2,1)S(1)}, bf16[2,128,1024]{2,1,0:T(8,128)(2,1)S(1)}, u32[]{:S(2)}, u32[]{:S(2)}) collective-permute-start(bf16[2,128,1024]{2,1,0:T(8,128)(2,1)S(1)} %collective-permute-done.10.refs_5_), channel_id=1, source_target_pairs={{0,4},{4,0},{8,12},{12,8},{16,20},{20,16},{24,28},{28,24},{1,5},{5... | collective-permute-start | bytes 1572872 | tf_op jit(solution)/shard_map/ppermute | solution.py:270
  114.7 12.9 %collective-permute-start.9 = (bf16[2,128,1024]{2,1,0:T(8,128)(2,1)S(1)}, bf16[2,128,1024]{2,1,0:T(8,128)(2,1)S(1)}, u32[]{:S(2)}, u32[]{:S(2)}) collective-permute-start(bf16[2,128,1024]{2,1,0:T(8,128)(2,1)S(1)} %collective-permute-done.6.refs_0_), channel_id=1, source_target_pairs={{0,1},{1,0},{2,3},{3,2},{4,5},{5,4},{6,7},{7,6},{8,9},{9,8},{10,11... | collective-permute-start | bytes 1572872 | tf_op jit(solution)/shard_map/ppermute | solution.py:274
  133.7 28.3 %collective-permute-start.12 = (bf16[2,256,3072]{2,1,0:T(8,128)(2,1)S(1)}, bf16[2,256,3072]{2,1,0:T(8,128)(2,1)S(1)}, u32[]{:S(2)}, u32[]{:S(2)}) collective-permute-start(bf16[2,256,3072]{2,1,0:T(8,128)(2,1)S(1)} %get-tuple-element.23.refs_1_), channel_id=1, source_target_pairs={{0,2},{2,0},{1,3},{3,1},{4,6},{6,4},{5,7},{7,5},{8,10},{10,8},{9,1... | collective-permute-start | bytes 9437192 | tf_op jit(solution)/shard_map/ppermute | solution.py:291
  133.8 13.2 %collective-permute-start.18 = (bf16[2,128,3072]{2,1,0:T(8,128)(2,1)S(1)}, bf16[2,128,3072]{2,1,0:T(8,128)(2,1)S(1)}, u32[]{:S(2)}, u32[]{:S(2)}) collective-permute-start(bf16[2,128,3072]{2,1,0:T(8,128)(2,1)S(1)} %get-tuple-element.19.packet_ref.refs_1_), channel_id=1, source_target_pairs={{0,2},{2,0},{1,3},{3,1},{4,6},{6,4},{5,7},{7,5},{8,10},{10,8},{9,1... | collective-permute-start | bytes 4718600 | tf_op jit(solution)/shard_map/ppermute | solution.py:291
  137.8 8.4 %collective-permute-start.3 = (bf16[128,1024]{1,0:T(8,128)(2,1)S(1)}, bf16[128,1024]{1,0:T(8,128)(2,1)S(1)}, u32[]{:S(2)}, u32[]{:S(2)}) collective-permute-start(bf16[128,1024]{1,0:T(8,128)(2,1)S(1)} %slice_bitcast_fusion), channel_id=1, source_target_pairs={{0,1},{1,0},{2,3},{3,2},{4,5},{5,4},{6,7},{7,6},{8,9},{9,8},{10,11... | collective-permute-start | bytes 786440 | tf_op jit(solution)/shard_map/ppermute | solution.py:298

commit v2 on v1

--- a/solution.py
+++ b/solution.py
@@ -181,7 +181,15 @@
 
 def accumulate_kernel(count, first, last, *refs):
     pieces = triples(refs, count)
-    up_ref, down_ref = refs[-2:]
+    if last:
+        *refs, here_ref, passed_ref, up_ref, down_ref, inputs_ref = refs
+
+        @pl.when(pl.program_id(0) == 0)
+        def _():
+            inputs_ref[...] = (here_ref[0].astype(F32) + passed_ref[...].astype(F32)).astype(BF16)
+
+    else:
+        up_ref, down_ref = refs[-2:]
     up_in, down_in = (None, None) if first else refs[3 * count : 3 * count + 2]
     hidden = down_ref.shape[0] if first else down_in.shape[0]
     tile = down_ref.shape[0] if last else tile_of(hidden)
@@ -200,20 +208,23 @@
         pl.loop(0, hidden // tile)(lambda step: add(step, lambda cols: cols, lambda cols: cols))
 
 
-def accumulate(pieces, sums, last):
+def accumulate(pieces, sums, last, parts):
     keep, packet, _ = pieces[0]
     tokens = sum(piece[0].shape[1] for piece in pieces)
     part = keep.shape[2]
     hidden = packet.shape[2] - part
     tile = tile_of(hidden)
     args = [array for piece in pieces for array in piece] + list(sums or ())
+    if last:
+        args += parts
     how = dict(
         in_specs=[VMEM] * len(args),
         out_specs=[VMEM, VMEM],
         out_shape=[
             jax.ShapeDtypeStruct((part, hidden), F32 if last else BF16),
             jax.ShapeDtypeStruct((hidden, part), F32 if last else BF16),
-        ],
+        ]
+        + [jax.ShapeDtypeStruct(t.shape, t.dtype) for t in parts[1:] if last],
         compiler_params=pltpu.CompilerParams(vmem_limit_bytes=(12 if last else 7) * MIB),
         cost_estimate=pl.CostEstimate(
             flops=8 * tokens * part * hidden, bytes_accessed=8 * part * hidden, transcendentals=0
@@ -226,6 +237,7 @@
             out_specs=[
                 pl.BlockSpec((part, tile), lambda j: (0, j)),
                 pl.BlockSpec((tile, part), lambda j: (j, 0)),
+                pl.BlockSpec(parts[1].shape, lambda j: (0, 0)),
             ],
         )
     elif sums is not None:
@@ -289,14 +301,13 @@
             if at == 0:
                 weights = (w_up, w_down, *more)
             made.append((keep, packet, lax.ppermute(packet, "fs", swap)))
+        partial_value = inputs_part(flag, made[0][1], rows, w_up, weights[2])
+        passed = lax.ppermute(partial_value[1], "tp", swap)
         sums = None
         for at, chunks in enumerate(BATCHES):
-            sums = accumulate([made[k] for k in chunks], sums, at == len(BATCHES) - 1)
-        grad_up, grad_down = sums
-
-        partial_value = inputs_part(flag, made[0][1], rows, w_up, weights[2])
-        passed = lax.ppermute(partial_value[1], "tp", swap)
-        grad_inputs = (partial_value[0].astype(F32) + passed.astype(F32)).astype(BF16)
+            sums = accumulate([made[k] for k in chunks], sums, at == len(BATCHES) - 1, [partial_value, passed])
+        grad_up, grad_down, grad_inputs = sums
+
         if n_rep > group:
             sets = [[base * group + at for base in range(n_rep // group)] for at in range(group)]
             grad_up, grad_down = (

time: 169 us -> 165 us (0.976)
  waiting for transfers between devices: 69.7 us -> 65.2 us
    ppermute x1, waiting for transfers between devices: 7.75 us -> 0.01 us  [shards(): passed = lax.ppermute(partial_value[1], 'tp', swap)]
    ppermute x4, waiting for transfers between devices: 0.01 us -> 3.27 us  [shards(): made.append((keep, packet, lax.ppermute(packet, 'fs', swap)))]
  transfers between devices with their start and end apart: 22 -> 22, of which waited for: 9 -> 9; matrix products, arithmetic and copies ran while one was open for 1% -> 1% of each run, Pallas kernels for 22% -> 23%
where the time goes in v2:
time: 165 us; the launch traced here: 164 us
  waiting for transfers between devices  65.2 us (40%)
  Pallas kernels  54 us (33%)
  starting transfers between devices  31.1 us (19%)
  local copies, waits for them, and re-layouts  11.5 us (7%)
    pallas_call x4, Pallas kernels, forward(): pl.pallas_call(functools.partial(forward_kernel, count, first), in_specs=...  28 us
    pallas_call x3, Pallas kernels, accumulate(): pl.pallas_call(functools.partial(accumulate_kernel, len(pieces), sums is...  22 us
    ppermute x3, starting transfers between devices, shards(): near[step] = lax.ppermute(near[step - 1], 'rep', along)  16.9 us
    ppermute x2, waiting for transfers between devices, shards(): over[step] = lax.ppermute(near[step], 'rep', across)  13.4 us
    ppermute x3, waiting for transfers between devices, shards(): near[step] = lax.ppermute(near[step - 1], 'rep', along)  13.2 us
    ppermute x1, waiting for transfers between devices, shards(): over = {0: lax.ppermute(near[0], 'rep', across)}  11.7 us
    unnamed x12, local copies, waits for them, and re-layouts  11.5 us
    ppermute x1, waiting for transfers between devices, shards(): corner = {0: lax.ppermute(beside[0], 'rep', across)}  11.2 us
  transfers between devices with their start and end apart: 22, of which 9 were waited for; matrix products, arithmetic and copies ran while one was open for 1% of the time, Pallas kernels for 23%

profile of v2, /device:TPU:0, one launch (start us, length us, event | category | flops | bytes accessed | tf_op | source)
XLA Modules:
  0.0 163.7 jit_solution(16993436140524558686)
XLA Ops:
  1.3 1.1 pad_maximum_fusion.refs_0_
  2.4 3.0 %collective-permute-start = (bf16[2,128,1024]{2,1,0:T(8,128)(2,1)S(1)}, bf16[2,128,1024]{2,1,0:T(8,128)(2,1)S(1)}, u32[]{:S(2)}, u32[]{:S(2)}) collective-permute-start(bf16[2,128,1024]{2,1,0:T(8,128)(2,1)S(1)} %pad_maximum_fusion.refs_0_), channel_id=1, source_target_pairs={{0,8},{4,12},{8,24},{12,28},{16,0},{20,4},{24,16},{28,20},{1,9},{5... | collective-permute-start | bytes 1572872 | tf_op jit(solution)/shard_map/ppermute | solution.py:278
  5.4 1.5 collective-permute-start.6
  6.9 11.7 %collective-permute-done.refs_0_ = bf16[2,128,1024]{2,1,0:T(8,128)(2,1)S(1)} collective-permute-done((bf16[2,128,1024]{2,1,0:T(8,128)(2,1)S(1)}, bf16[2,128,1024]{2,1,0:T(8,128)(2,1)S(1)}, u32[]{:S(2)}, u32[]{:S(2)}) %collective-permute-start) | collective-permute-done | bytes 524320 | tf_op jit(solution)/shard_map/ppermute | solution.py:278
  18.6 1.6 collective-permute-start.12
  20.9 2.1 %collective-permute-start.7 = (bf16[2,128,1024]{2,1,0:T(8,128)(2,1)S(1)}, bf16[2,128,1024]{2,1,0:T(8,128)(2,1)S(1)}, u32[]{:S(2)}, u32[]{:S(2)}) collective-permute-start(bf16[2,128,1024]{2,1,0:T(8,128)(2,1)S(1)} %collective-permute-done.6.refs_1_), channel_id=1, source_target_pairs={{8,0},{12,4},{24,8},{28,12},{0,16},{4,20},{16,24},{20,28},{9,1},{1... | collective-permute-start | bytes 1572872 | tf_op jit(solution)/shard_map/ppermute | solution.py:280
  23.1 8.8 %collective-permute-done.12.refs_1_ = bf16[2,128,1024]{2,1,0:T(8,128)(2,1)S(1)} collective-permute-done((bf16[2,128,1024]{2,1,0:T(8,128)(2,1)S(1)}, bf16[2,128,1024]{2,1,0:T(8,128)(2,1)S(1)}, u32[]{:S(2)}, u32[]{:S(2)}) %collective-permute-start.12) | collective-permute-done | bytes 524320 | tf_op jit(solution)/shard_map/ppermute | solution.py:285
  31.9 1.3 collective-permute-start.15
  33.2 1.5 collective-permute-done.1.refs_0_
  34.7 1.5 collective-permute-start.14
  36.2 2.0 %copy-done.4 = bf16[2048,1024]{1,0:T(8,128)(2,1)} copy-done((bf16[2048,1024]{1,0:T(8,128)(2,1)}, bf16[2048,1024]{1,0:T(8,128)(2,1)S(1)}, u32[]{:S(2)}) %copy-start.4) | copy-done | bytes 4194328
  38.2 13.1 %collective-permute-start.13 = (bf16[2,128,1024]{2,1,0:T(8,128)(2,1)S(1)}, bf16[2,128,1024]{2,1,0:T(8,128)(2,1)}, u32[]{:S(2)}, u32[]{:S(2)}) collective-permute-start(bf16[2,128,1024]{2,1,0:T(8,128)(2,1)S(1)} %collective-permute-done.1.refs_0_), channel_id=1, source_target_pairs={{0,8},{4,12},{8,24},{12,28},{16,0},{20,4},{24,16},{28,20},{1,9},{5... | collective-permute-start | bytes 1572872 | tf_op jit(solution)/shard_map/ppermute | solution.py:278
  51.3 2.2 %copy-done = bf16[1024,2048]{1,0:T(8,128)(2,1)S(1)} copy-done((bf16[1024,2048]{1,0:T(8,128)(2,1)S(1)}, bf16[1024,2048]{1,0:T(8,128)(2,1)}, u32[]{:S(2)}) %copy-start) | copy-done | bytes 4194328
  53.4 2.2 %copy-done.2 = bf16[2048,1024]{1,0:T(8,128)(2,1)S(1)} copy-done((bf16[2048,1024]{1,0:T(8,128)(2,1)S(1)}, bf16[2048,1024]{1,0:T(8,128)(2,1)}, u32[]{:S(2)}) %copy-start.2) | copy-done | bytes 4194328
  56.2 1.6 %copy-done.1 = bf16[1024,2048]{1,0:T(8,128)(2,1)S(1)} copy-done((bf16[1024,2048]{1,0:T(8,128)(2,1)S(1)}, bf16[1024,2048]{1,0:T(8,128)(2,1)}, u32[]{:S(2)}) %copy-start.1) | copy-done | bytes 4194328
  57.8 1.3 copy-done.3
  59.1 2.2 %copy-done.5 = bf16[2048,1024]{1,0:T(8,128)(2,1)S(1)} copy-done((bf16[2048,1024]{1,0:T(8,128)(2,1)S(1)}, bf16[2048,1024]{1,0:T(8,128)(2,1)}, u32[]{:S(2)}) %copy-start.5) | copy-done | bytes 4194328
  61.3 6.5 %forward.4 = (bf16[2,128,3072]{2,1,0:T(8,128)(2,1)S(1)}, bf16[2,128,1024]{2,1,0:T(8,128)(2,1)S(1)}, bf16[1024,2048]{1,0:T(8,128)(2,1)S(1)}, bf16[2048,1024]{1,0:T(8,128)(2,1)S(1)}) custom-call(s32[1]{0:T(128)} %ready.1.same_ref, bf16[2,128,1024]{2,1,0:T(8,128)(2,1)S(1)} %pad_maximum_fusion.refs_0_, bf16[2,128,1024]{2,1,0:T(8,128)(2,1)S(1)} %collective-permute-done.6.refs_1_, ...), custom_call_target="tpu_custom_call" | custom-call | flops 2147483648 | bytes 16777216 | tf_op jit(solution)/shard_map/forward/pallas_call | solution.py:122
  67.8 9.5 %forward.6 = (bf16[2,384,3072]{2,1,0:T(8,128)(2,1)S(1)}, bf16[2,384,1024]{2,1,0:T(8,128)(2,1)S(1)}) custom-call(s32[1]{0:T(128)} %ready.1.same_ref, bf16[2,128,1024]{2,1,0:T(8,128)(2,1)S(1)} %collective-permute-done.1.refs_0_, bf16[2,128,1024]{2,1,0:T(8,128)(2,1)S(1)} %collective-permute-done.12.refs_1_, ...), custom_call_target="tpu_custom_call" | custom-call | flops 6442450944 | bytes 16777216 | tf_op jit(solution)/shard_map/forward/pallas_call | solution.py:122
  78.0 1.5 collective-permute-start.19
  80.6 11.7 %collective-permute-done.3.refs_1_ = bf16[2,128,1024]{2,1,0:T(8,128)(2,1)S(1)} collective-permute-done((bf16[2,128,1024]{2,1,0:T(8,128)(2,1)S(1)}, bf16[2,128,1024]{2,1,0:T(8,128)(2,1)S(1)}, u32[]{:S(2)}, u32[]{:S(2)}) %collective-permute-start.3) | collective-permute-done | bytes 524320 | tf_op jit(solution)/shard_map/ppermute | solution.py:275
  92.3 11.2 %collective-permute-done.19.refs_3_ = bf16[2,128,1024]{2,1,0:T(8,128)(2,1)S(1)} collective-permute-done((bf16[2,128,1024]{2,1,0:T(8,128)(2,1)S(1)}, bf16[2,128,1024]{2,1,0:T(8,128)(2,1)S(1)}, u32[]{:S(2)}, u32[]{:S(2)}) %collective-permute-start.19) | collective-permute-done | bytes 524320 | tf_op jit(solution)/shard_map/ppermute | solution.py:276
  103.5 5.9 %forward.7 = (bf16[2,256,3072]{2,1,0:T(8,128)(2,1)S(1)}, bf16[2,256,1024]{2,1,0:T(8,128)(2,1)S(1)}) custom-call(s32[1]{0:T(128)} %ready.1.same_ref, bf16[2,128,1024]{2,1,0:T(8,128)(2,1)S(1)} %collective-permute-done.refs_0_, bf16[2,128,1024]{2,1,0:T(8,128)(2,1)S(1)} %collective-permute-done.3.refs_1_, ...), custom_call_target="tpu_custom_call" | custom-call | flops 4294967296 | bytes 16777216 | tf_op jit(solution)/shard_map/forward/pallas_call | solution.py:122
  110.2 4.6 %collective-permute-done.2.refs_0_ = bf16[2,128,1024]{2,1,0:T(8,128)(2,1)S(1)} collective-permute-done((bf16[2,128,1024]{2,1,0:T(8,128)(2,1)S(1)}, bf16[2,128,1024]{2,1,0:T(8,128)(2,1)S(1)}, u32[]{:S(2)}, u32[]{:S(2)}) %collective-permute-start.2) | collective-permute-done | bytes 524320 | tf_op jit(solution)/shard_map/ppermute | solution.py:285
  115.3 10.2 %collective-permute-done.4.refs_1_ = bf16[2,128,1024]{2,1,0:T(8,128)(2,1)S(1)} collective-permute-done((bf16[2,128,1024]{2,1,0:T(8,128)(2,1)S(1)}, bf16[2,128,1024]{2,1,0:T(8,128)(2,1)S(1)}, u32[]{:S(2)}, u32[]{:S(2)}) %collective-permute-start.4) | collective-permute-done | bytes 524320 | tf_op jit(solution)/shard_map/ppermute | solution.py:281
  125.5 2.1 %collective-permute-done.5.refs_2_ = bf16[2,128,1024]{2,1,0:T(8,128)(2,1)S(1)} collective-permute-done((bf16[2,128,1024]{2,1,0:T(8,128)(2,1)S(1)}, bf16[2,128,1024]{2,1,0:T(8,128)(2,1)S(1)}, u32[]{:S(2)}, u32[]{:S(2)}) %collective-permute-start.5) | collective-permute-done | bytes 524320 | tf_op jit(solution)/shard_map/ppermute | solution.py:286
  127.6 6.1 %forward.5 = (bf16[2,256,3072]{2,1,0:T(8,128)(2,1)S(1)}, bf16[2,256,1024]{2,1,0:T(8,128)(2,1)S(1)}) custom-call(s32[1]{0:T(128)} %ready.1.same_ref, bf16[2,128,1024]{2,1,0:T(8,128)(2,1)S(1)} %collective-permute-done.2.refs_0_, bf16[2,128,1024]{2,1,0:T(8,128)(2,1)S(1)} %collective-permute-done.4.refs_1_, ...), custom_call_target="tpu_custom_call" | custom-call | flops 4294967296 | bytes 16777216 | tf_op jit(solution)/shard_map/forward/pallas_call | solution.py:122
  134.3 3.5 %inputs_part.1.refs_5_ = bf16[2,128,1024]{2,1,0:T(8,128)(2,1)S(1)} custom-call(s32[1]{0:T(128)} %ready.1.same_ref, bf16[2,128,3072]{2,1,0:T(8,128)(2,1)S(1)} %get-tuple-element.27.refs_1_.packet_ref, bf16[1024,2048]{1,0:T(8,128)(2,1)S(1)} %copy-done.1, bf16[1024,2048]{1,0:T(8,128)(2,1)S(1)} %get-tuple-element.20.refs_6_.refs_8_.up_other), custom_call_target="tpu_custom_call" | custom-call | flops 1073741824 | bytes 8388608 | tf_op jit(solution)/shard_map/inputs_part/pallas_call | solution.py:149
  138.4 3.3 %collective-permute-done.17.refs_2_ = bf16[2,128,3072]{2,1,0:T(8,128)(2,1)S(1)} collective-permute-done((bf16[2,128,3072]{2,1,0:T(8,128)(2,1)S(1)}, bf16[2,128,3072]{2,1,0:T(8,128)(2,1)S(1)}, u32[]{:S(2)}, u32[]{:S(2)}) %collective-permute-start.17) | collective-permute-done | bytes 1572896 | tf_op jit(solution)/shard_map/ppermute | solution.py:303
  141.7 7.4 %accumulate.3 = (bf16[1024,2048]{1,0:T(8,128)(2,1)S(1)}, bf16[2048,1024]{1,0:T(8,128)(2,1)S(1)}) custom-call(bf16[2,128,1024]{2,1,0:T(8,128)(2,1)S(1)} %get-tuple-element.26.refs_0_, bf16[2,128,3072]{2,1,0:T(8,128)(2,1)S(1)} %get-tuple-element.27.refs_1_.packet_ref, bf16[2,128,3072]{2,1,0:T(8,128)(2,1)S(1)} %collective-permute-done.17.refs_2_, ...), custom_call_target="tpu_custom_call" | custom-call | flops 6442450944 | bytes 16777216 | tf_op jit(solution)/shard_map/accumulate/pallas_call | solution.py:245
  149.1 7.7 %accumulate.4 = (bf16[1024,2048]{1,0:T(8,128)(2,1)S(1)}, bf16[2048,1024]{1,0:T(8,128)(2,1)S(1)}) custom-call(bf16[2,384,1024]{2,1,0:T(8,128)(2,1)S(1)} %get-tuple-element.24.refs_0_, bf16[2,384,3072]{2,1,0:T(8,128)(2,1)S(1)} %get-tuple-element.25.refs_1_, ...), custom_call_target="tpu_custom_call", output_to_operand_aliasing={{0}: (3, {}), {1}: (4, {})} | custom-call | flops 6442450944 | bytes 16777216 | tf_op jit(solution)/shard_map/accumulate/pallas_call | solution.py:245
  156.8 6.9 %accumulate.5 = (f32[1024,2048]{1,0:T(8,128)}, f32[2048,1024]{1,0:T(8,128)}, bf16[128,1024]{1,0:T(8,128)(2,1)}) custom-call(bf16[2,256,1024]{2,1,0:T(8,128)(2,1)S(1)} %get-tuple-element.22.refs_0_, bf16[2,256,3072]{2,1,0:T(8,128)(2,1)S(1)} %get-tuple-element.23.refs_1_, bf16[2,256,3072]{2,1,0:T(8,128)(2,1)S(1)} %collective-permute-done.11.refs_2_, ...), custom_call_target="tpu_custom_call" | custom-call | flops 4294967296 | bytes 16777216 | tf_op jit(solution)/shard_map/accumulate/pallas_call | solution.py:245
  (35 shorter events, 6.1 us)
Async XLA Ops:
  0.6 35.5 %collective-permute-start.10 = (bf16[2048,1024]{1,0:T(8,128)(2,1)}, bf16[2048,1024]{1,0:T(8,128)(2,1)S(1)}, u32[]{:S(2)}, u32[]{:S(2)}) collective-permute-start(bf16[2048,1024]{1,0:T(8,128)(2,1)} %refs_5_.3), channel_id=1, source_target_pairs={{0,2},{2,0},{1,3},{3,1},{4,6},{6,4},{5,7},{7,5},{8,10},{10,8},{9,1... | collective-permute-start | bytes 12582920 | tf_op jit(solution)/shard_map/ppermute | solution.py:288
  1.2 55.0 %collective-permute-start.9 = (bf16[1024,2048]{1,0:T(8,128)(2,1)}, bf16[1024,2048]{1,0:T(8,128)(2,1)}, u32[]{:S(2)}, u32[]{:S(2)}) collective-permute-start(bf16[1024,2048]{1,0:T(8,128)(2,1)} %up_ref.3), channel_id=1, source_target_pairs={{0,2},{2,0},{1,3},{3,1},{4,6},{6,4},{5,7},{7,5},{8,10},{10,8},{9,1... | collective-permute-start | bytes 12582920 | tf_op jit(solution)/shard_map/ppermute | solution.py:287
  2.4 16.2 %collective-permute-start = (bf16[2,128,1024]{2,1,0:T(8,128)(2,1)S(1)}, bf16[2,128,1024]{2,1,0:T(8,128)(2,1)S(1)}, u32[]{:S(2)}, u32[]{:S(2)}) collective-permute-start(bf16[2,128,1024]{2,1,0:T(8,128)(2,1)S(1)} %pad_maximum_fusion.refs_0_), channel_id=1, source_target_pairs={{0,8},{4,12},{8,24},{12,28},{16,0},{20,4},{24,16},{28,20},{1,9},{5... | collective-permute-start | bytes 1572872 | tf_op jit(solution)/shard_map/ppermute | solution.py:278
  5.4 15.5 %collective-permute-start.6 = (bf16[2,128,1024]{2,1,0:T(8,128)(2,1)S(1)}, bf16[2,128,1024]{2,1,0:T(8,128)(2,1)S(1)}, u32[]{:S(2)}, u32[]{:S(2)}) collective-permute-start(bf16[2,128,1024]{2,1,0:T(8,128)(2,1)S(1)} %pad_maximum_fusion.refs_0_), channel_id=1, source_target_pairs={{0,1},{1,0},{2,3},{3,2},{4,5},{5,4},{6,7},{7,6},{8,9},{9,8},{10,11... | collective-permute-start | bytes 1572872 | tf_op jit(solution)/shard_map/ppermute | solution.py:274
  18.6 13.3 %collective-permute-start.12 = (bf16[2,128,1024]{2,1,0:T(8,128)(2,1)S(1)}, bf16[2,128,1024]{2,1,0:T(8,128)(2,1)S(1)}, u32[]{:S(2)}, u32[]{:S(2)}) collective-permute-start(bf16[2,128,1024]{2,1,0:T(8,128)(2,1)S(1)} %collective-permute-done.refs_0_), channel_id=1, source_target_pairs={{0,4},{4,0},{8,12},{12,8},{16,20},{20,16},{24,28},{28,24},{1,5},{5... | collective-permute-start | bytes 1572872 | tf_op jit(solution)/shard_map/ppermute | solution.py:285
  20.1 14.5 %collective-permute-start.1 = (bf16[2,128,1024]{2,1,0:T(8,128)(2,1)S(1)}, bf16[2,128,1024]{2,1,0:T(8,128)(2,1)S(1)}, u32[]{:S(2)}, u32[]{:S(2)}) collective-permute-start(bf16[2,128,1024]{2,1,0:T(8,128)(2,1)S(1)} %collective-permute-done.refs_0_), channel_id=1, source_target_pairs={{0,8},{4,12},{8,24},{12,28},{16,0},{20,4},{24,16},{28,20},{1,9},{5... | collective-permute-start | bytes 1572872 | tf_op jit(solution)/shard_map/ppermute | solution.py:278
  20.9 46.8 %collective-permute-start.7 = (bf16[2,128,1024]{2,1,0:T(8,128)(2,1)S(1)}, bf16[2,128,1024]{2,1,0:T(8,128)(2,1)S(1)}, u32[]{:S(2)}, u32[]{:S(2)}) collective-permute-start(bf16[2,128,1024]{2,1,0:T(8,128)(2,1)S(1)} %collective-permute-done.6.refs_1_), channel_id=1, source_target_pairs={{8,0},{12,4},{24,8},{28,12},{0,16},{4,20},{16,24},{20,28},{9,1},{1... | collective-permute-start | bytes 1572872 | tf_op jit(solution)/shard_map/ppermute | solution.py:280
  31.9 35.9 %collective-permute-start.15 = (bf16[2,128,1024]{2,1,0:T(8,128)(2,1)S(1)}, bf16[2,128,1024]{2,1,0:T(8,128)(2,1)}, u32[]{:S(2)}, u32[]{:S(2)}) collective-permute-start(bf16[2,128,1024]{2,1,0:T(8,128)(2,1)S(1)} %collective-permute-done.12.refs_1_), channel_id=1, source_target_pairs={{0,1},{1,0},{2,3},{3,2},{4,5},{5,4},{6,7},{7,6},{8,9},{9,8},{10,11... | collective-permute-start | bytes 1572872 | tf_op jit(solution)/shard_map/ppermute | solution.py:286
  34.7 33.1 %collective-permute-start.14 = (bf16[2,128,1024]{2,1,0:T(8,128)(2,1)S(1)}, bf16[2,128,1024]{2,1,0:T(8,128)(2,1)}, u32[]{:S(2)}, u32[]{:S(2)}) collective-permute-start(bf16[2,128,1024]{2,1,0:T(8,128)(2,1)S(1)} %collective-permute-done.1.refs_0_), channel_id=1, source_target_pairs={{0,1},{1,0},{2,3},{3,2},{4,5},{5,4},{6,7},{7,6},{8,9},{9,8},{10,11... | collective-permute-start | bytes 1572872 | tf_op jit(solution)/shard_map/ppermute | solution.py:284
  36.2 2.0 %copy-start.4 = (bf16[2048,1024]{1,0:T(8,128)(2,1)}, bf16[2048,1024]{1,0:T(8,128)(2,1)S(1)}, u32[]{:S(2)}) copy-start(bf16[2048,1024]{1,0:T(8,128)(2,1)S(1)} %collective-permute-done.10.refs_5_) | copy-start | bytes 12582916
  38.2 29.6 %collective-permute-start.13 = (bf16[2,128,1024]{2,1,0:T(8,128)(2,1)S(1)}, bf16[2,128,1024]{2,1,0:T(8,128)(2,1)}, u32[]{:S(2)}, u32[]{:S(2)}) collective-permute-start(bf16[2,128,1024]{2,1,0:T(8,128)(2,1)S(1)} %collective-permute-done.1.refs_0_), channel_id=1, source_target_pairs={{0,8},{4,12},{8,24},{12,28},{16,0},{20,4},{24,16},{28,20},{1,9},{5... | collective-permute-start | bytes 1572872 | tf_op jit(solution)/shard_map/ppermute | solution.py:278
  51.2 2.2 %copy-start = (bf16[1024,2048]{1,0:T(8,128)(2,1)S(1)}, bf16[1024,2048]{1,0:T(8,128)(2,1)}, u32[]{:S(2)}) copy-start(bf16[1024,2048]{1,0:T(8,128)(2,1)} %up_ref.3) | copy-start | bytes 12582916
  53.4 2.2 %copy-start.2 = (bf16[2048,1024]{1,0:T(8,128)(2,1)S(1)}, bf16[2048,1024]{1,0:T(8,128)(2,1)}, u32[]{:S(2)}) copy-start(bf16[2048,1024]{1,0:T(8,128)(2,1)} %refs_5_.3) | copy-start | bytes 12582916
  55.6 2.2 %copy-start.1 = (bf16[1024,2048]{1,0:T(8,128)(2,1)S(1)}, bf16[1024,2048]{1,0:T(8,128)(2,1)}, u32[]{:S(2)}) copy-start(bf16[1024,2048]{1,0:T(8,128)(2,1)} %up_ref.3) | copy-start | bytes 12582916
  55.6 3.5 %copy-start.3 = (bf16[2048,1024]{1,0:T(8,128)(2,1)S(1)}, bf16[2048,1024]{1,0:T(8,128)(2,1)}, u32[]{:S(2)}) copy-start(bf16[2048,1024]{1,0:T(8,128)(2,1)} %refs_5_.3) | copy-start | bytes 12582916
  59.1 2.2 %copy-start.5 = (bf16[2048,1024]{1,0:T(8,128)(2,1)S(1)}, bf16[2048,1024]{1,0:T(8,128)(2,1)}, u32[]{:S(2)}) copy-start(bf16[2048,1024]{1,0:T(8,128)(2,1)} %copy-done.4) | copy-start | bytes 12582916
  77.3 71.8 %collective-permute-start.16 = (bf16[2,384,3072]{2,1,0:T(8,128)(2,1)S(1)}, bf16[2,384,3072]{2,1,0:T(8,128)(2,1)S(1)}, u32[]{:S(2)}, u32[]{:S(2)}) collective-permute-start(bf16[2,384,3072]{2,1,0:T(8,128)(2,1)S(1)} %get-tuple-element.25.refs_1_), channel_id=1, source_target_pairs={{0,2},{2,0},{1,3},{3,1},{4,6},{6,4},{5,7},{7,5},{8,10},{10,8},{9,1... | collective-permute-start | bytes 14155784 | tf_op jit(solution)/shard_map/ppermute | solution.py:303
  77.4 14.9 %collective-permute-start.3 = (bf16[2,128,1024]{2,1,0:T(8,128)(2,1)S(1)}, bf16[2,128,1024]{2,1,0:T(8,128)(2,1)S(1)}, u32[]{:S(2)}, u32[]{:S(2)}) collective-permute-start(bf16[2,128,1024]{2,1,0:T(8,128)(2,1)S(1)} %pad_maximum_fusion.refs_0_), channel_id=1, source_target_pairs={{0,4},{4,0},{8,12},{12,8},{16,20},{20,16},{24,28},{28,24},{1,5},{5... | collective-permute-start | bytes 1572872 | tf_op jit(solution)/shard_map/ppermute | solution.py:275
  78.0 25.5 %collective-permute-start.19 = (bf16[2,128,1024]{2,1,0:T(8,128)(2,1)S(1)}, bf16[2,128,1024]{2,1,0:T(8,128)(2,1)S(1)}, u32[]{:S(2)}, u32[]{:S(2)}) collective-permute-start(bf16[2,128,1024]{2,1,0:T(8,128)(2,1)S(1)} %collective-permute-done.6.refs_1_), channel_id=1, source_target_pairs={{0,4},{4,0},{8,12},{12,8},{16,20},{20,16},{24,28},{28,24},{1,5},{5... | collective-permute-start | bytes 1572872 | tf_op jit(solution)/shard_map/ppermute | solution.py:276
  79.5 24.0 %collective-permute-start.18 = (bf16[2,128,1024]{2,1,0:T(8,128)(2,1)S(1)}, bf16[2,128,1024]{2,1,0:T(8,128)(2,1)S(1)}, u32[]{:S(2)}, u32[]{:S(2)}) collective-permute-start(bf16[2,128,1024]{2,1,0:T(8,128)(2,1)S(1)} %collective-permute-done.refs_0_), channel_id=1, source_target_pairs={{0,1},{1,0},{2,3},{3,2},{4,5},{5,4},{6,7},{7,6},{8,9},{9,8},{10,11... | collective-permute-start | bytes 1572872 | tf_op jit(solution)/shard_map/ppermute | solution.py:284
  80.0 34.7 %collective-permute-start.2 = (bf16[2,128,1024]{2,1,0:T(8,128)(2,1)S(1)}, bf16[2,128,1024]{2,1,0:T(8,128)(2,1)S(1)}, u32[]{:S(2)}, u32[]{:S(2)}) collective-permute-start(bf16[2,128,1024]{2,1,0:T(8,128)(2,1)S(1)} %collective-permute-done.1.refs_0_), channel_id=1, source_target_pairs={{0,4},{4,0},{8,12},{12,8},{16,20},{20,16},{24,28},{28,24},{1,5},{5... | collective-permute-start | bytes 1572872 | tf_op jit(solution)/shard_map/ppermute | solution.py:285
  109.4 32.3 %collective-permute-start.20 = (bf16[2,256,3072]{2,1,0:T(8,128)(2,1)S(1)}, bf16[2,256,3072]{2,1,0:T(8,128)(2,1)S(1)}, u32[]{:S(2)}, u32[]{:S(2)}) collective-permute-start(bf16[2,256,3072]{2,1,0:T(8,128)(2,1)S(1)} %get-tuple-element.29.refs_4_), channel_id=1, source_target_pairs={{0,2},{2,0},{1,3},{3,1},{4,6},{6,4},{5,7},{7,5},{8,10},{10,8},{9,1... | collective-permute-start | bytes 9437192 | tf_op jit(solution)/shard_map/ppermute | solution.py:303
  109.5 16.0 %collective-permute-start.4 = (bf16[2,128,1024]{2,1,0:T(8,128)(2,1)S(1)}, bf16[2,128,1024]{2,1,0:T(8,128)(2,1)S(1)}, u32[]{:S(2)}, u32[]{:S(2)}) collective-permute-start(bf16[2,128,1024]{2,1,0:T(8,128)(2,1)S(1)} %collective-permute-done.3.refs_1_), channel_id=1, source_target_pairs={{8,0},{12,4},{24,8},{28,12},{0,16},{4,20},{16,24},{20,28},{9,1},{1... | collective-permute-start | bytes 1572872 | tf_op jit(solution)/shard_map/ppermute | solution.py:281
  109.6 15.9 %collective-permute-start.8 = (bf16[2,128,1024]{2,1,0:T(8,128)(2,1)S(1)}, bf16[2,128,1024]{2,1,0:T(8,128)(2,1)S(1)}, u32[]{:S(2)}, u32[]{:S(2)}) collective-permute-start(bf16[2,128,1024]{2,1,0:T(8,128)(2,1)S(1)} %collective-permute-done.7.refs_5_), channel_id=1, source_target_pairs={{0,4},{4,0},{8,12},{12,8},{16,20},{20,16},{24,28},{28,24},{1,5},{5... | collective-permute-start | bytes 1572872 | tf_op jit(solution)/shard_map/ppermute | solution.py:282
  114.7 12.9 %collective-permute-start.5 = (bf16[2,128,1024]{2,1,0:T(8,128)(2,1)S(1)}, bf16[2,128,1024]{2,1,0:T(8,128)(2,1)S(1)}, u32[]{:S(2)}, u32[]{:S(2)}) collective-permute-start(bf16[2,128,1024]{2,1,0:T(8,128)(2,1)S(1)} %collective-permute-done.2.refs_0_), channel_id=1, source_target_pairs={{0,1},{1,0},{2,3},{3,2},{4,5},{5,4},{6,7},{7,6},{8,9},{9,8},{10,11... | collective-permute-start | bytes 1572872 | tf_op jit(solution)/shard_map/ppermute | solution.py:286
  133.7 23.1 %collective-permute-start.11 = (bf16[2,256,3072]{2,1,0:T(8,128)(2,1)S(1)}, bf16[2,256,3072]{2,1,0:T(8,128)(2,1)S(1)}, u32[]{:S(2)}, u32[]{:S(2)}) collective-permute-start(bf16[2,256,3072]{2,1,0:T(8,128)(2,1)S(1)} %get-tuple-element.23.refs_1_), channel_id=1, source_target_pairs={{0,2},{2,0},{1,3},{3,1},{4,6},{6,4},{5,7},{7,5},{8,10},{10,8},{9,1... | collective-permute-start | bytes 9437192 | tf_op jit(solution)/shard_map/ppermute | solution.py:303
  133.8 7.9 %collective-permute-start.17 = (bf16[2,128,3072]{2,1,0:T(8,128)(2,1)S(1)}, bf16[2,128,3072]{2,1,0:T(8,128)(2,1)S(1)}, u32[]{:S(2)}, u32[]{:S(2)}) collective-permute-start(bf16[2,128,3072]{2,1,0:T(8,128)(2,1)S(1)} %get-tuple-element.27.refs_1_.packet_ref), channel_id=1, source_target_pairs={{0,2},{2,0},{1,3},{3,1},{4,6},{6,4},{5,7},{7,5},{8,10},{10,8},{9,1... | collective-permute-start | bytes 4718600 | tf_op jit(solution)/shard_map/ppermute | solution.py:303
  137.8 19.0 %collective-permute-start.21 = (bf16[128,1024]{1,0:T(8,128)(2,1)S(1)}, bf16[128,1024]{1,0:T(8,128)(2,1)S(1)}, u32[]{:S(2)}, u32[]{:S(2)}) collective-permute-start(bf16[128,1024]{1,0:T(8,128)(2,1)S(1)} %slice_bitcast_fusion), channel_id=1, source_target_pairs={{0,1},{1,0},{2,3},{3,2},{4,5},{5,4},{6,7},{7,6},{8,9},{9,8},{10,11... | collective-permute-start | bytes 786440 | tf_op jit(solution)/shard_map/ppermute | solution.py:305
